TPU v7x, 32 devices: a whole 2x2x4 slice. The times are simulated.
32 devices in a mesh: sp: 16 (over z, y, x), tp: 2 (over core).
Axes of the slice: x: 2, y: 2, z: 4, core: 2. Of those that a mesh axis runs over, the one named last changes fastest.
Arguments:
- hidden: bfloat16 [4096, 2048], P('sp', 'tp'), may hold values from -16 to 16
- query_weight: bfloat16 [2048, 1024], P(None, 'tp'), may hold values from -0.125 to 0.125
- key_weight: bfloat16 [2048, 512], P(None, 'tp'), may hold values from -0.125 to 0.125
- value_weight: bfloat16 [2048, 512], P(None, 'tp'), may hold values from -0.125 to 0.125
- head_gate_weight: bfloat16 [2048, 1024], P(None, 'tp'), may hold values from -0.125 to 0.125
- state_in_weight: bfloat16 [2048, 1024], P(None, 'tp'), may hold values from -0.125 to 0.125
- state_gate_weight: bfloat16 [2048, 1024], P(None, 'tp'), may hold values from -0.125 to 0.125
- sink_logit: float32 [16], P('tp'), may hold values from 1 to 6
- decay_real: float32 [64, 64], P('tp'), may hold values from -0.7 to -0.0049
- decay_frequency: float32 [64, 64], P('tp'), may hold values from 0 to 192
- log_step: float32 [64], P('tp'), may hold values from -20 to 0
- input_real: float32 [64, 64, 16], P('tp'), may hold values from -1028 to 1028
- input_imaginary: float32 [64, 64, 16], P('tp'), may hold values from -1028 to 1028
- output_real: float32 [64, 16, 64], P('tp'), may hold values from -0.5 to 0.5
- output_imaginary: float32 [64, 16, 64], P('tp'), may hold values from -0.5 to 0.5
- skip_weight: float32 [64, 16], P('tp'), may hold values from -3 to 3
- decay_shift: float32 [64, 4096], P('tp', 'sp'), may hold values from -2 to 0
- head_out_weight: bfloat16 [1024, 2048], P('tp'), may hold values from -0.375 to 0.375
- state_out_weight: bfloat16 [1024, 2048], P('tp'), may hold values from -0.375 to 0.375
Outputs:
- layer_out: bfloat16 [4096, 2048], P('sp', 'tp')
All inputs are finite; a program needn't handle non-finite values.
Results may differ from a plain program's by a relative error of at most 0.012.
Values may be sent and summed in bfloat16 or wider, within the bound.
A program may use at most 128 MiB of HBM per device.

v0:
```python
import jax
import jax.numpy as jnp
import numpy as np
from jax import lax
from jax.experimental import pallas as pl
from jax.experimental.pallas import tpu as pltpu
from jax.sharding import PartitionSpec as P

HEAD_DIM = 64
Q_HEADS = 16
KV_HEADS = 8
GROUP_CH = 16
WINDOW = 128
CHUNK = 16
LANES = 128

NEG_FILL = -1e30
MESH = pl.DeviceIdType.MESH
VMEM = pl.BlockSpec(memory_space=pltpu.VMEM)
BF16 = jnp.bfloat16
F32 = jnp.float32


def params(collective_id=None):
    extra = {} if collective_id is None else {"collective_id": collective_id, "has_side_effects": True}
    return pltpu.CompilerParams(vmem_limit_bytes=60 * 1024 * 1024, **extra)


def hidden_kernel(own_ref, full_ref, send_sem, recv_sem):
    me = lax.axis_index("tp")
    other = 1 - me
    width = own_ref.shape[1]
    barrier = pltpu.get_barrier_semaphore()
    pl.semaphore_signal(barrier, inc=1, device_id={"tp": other}, device_id_type=MESH)
    pl.semaphore_wait(barrier, 1)
    mine = pl.ds(pl.multiple_of(me * width, LANES), width)
    copy = pltpu.make_async_remote_copy(
        src_ref=own_ref,
        dst_ref=full_ref.at[:, mine],
        send_sem=send_sem,
        recv_sem=recv_sem,
        device_id={"tp": other},
        device_id_type=MESH,
    )
    copy.start()
    full_ref[:, mine] = own_ref[...]
    copy.wait()


def gather_hidden(hidden):
    rows, width = hidden.shape
    return pl.pallas_call(
        hidden_kernel,
        out_shape=jax.ShapeDtypeStruct((rows, 2 * width), hidden.dtype),
        in_specs=[VMEM],
        out_specs=VMEM,
        scratch_shapes=[pltpu.SemaphoreType.DMA, pltpu.SemaphoreType.DMA],
        compiler_params=params(0),
        name="hidden_exchange",
    )(hidden)


def output_kernel(head_ref, state_ref, how_ref, sow_ref, out_ref, away, landed, send_sem, recv_sem):
    me = lax.axis_index("tp")
    other = 1 - me
    rows, width = out_ref.shape
    pieces = away.shape[0]
    step = width // pieces
    barrier = pltpu.get_barrier_semaphore()
    pl.semaphore_signal(barrier, inc=1, device_id={"tp": other}, device_id_type=MESH)
    pl.semaphore_wait(barrier, 1)

    def product(owner, piece):
        columns = pl.ds(pl.multiple_of(owner * width + piece * step, LANES), step)
        return jnp.dot(head_ref[...], how_ref[:, columns], preferred_element_type=F32) + jnp.dot(
            state_ref[...], sow_ref[:, columns], preferred_element_type=F32
        )

    copies = [
        pltpu.make_async_remote_copy(
            src_ref=away.at[piece],
            dst_ref=landed.at[piece],
            send_sem=send_sem.at[piece],
            recv_sem=recv_sem.at[piece],
            device_id={"tp": other},
            device_id_type=MESH,
        )
        for piece in range(pieces)
    ]
    for piece in range(pieces):
        away[piece] = product(other, piece).astype(away.dtype)
        if piece > 0:
            copies[piece - 1].start()
    own = [product(me, 0)]
    copies[pieces - 1].start()
    for piece in range(pieces):
        total = own[0] if piece == 0 else product(me, piece)
        copies[piece].wait()
        out_ref[:, pl.ds(piece * step, step)] = (total + landed[piece].astype(F32)).astype(out_ref.dtype)


def project_out(head_mixed, state_mixed, head_out_weight, state_out_weight):
    rows = head_mixed.shape[0]
    width = head_out_weight.shape[1] // 2
    pieces = 4
    return pl.pallas_call(
        output_kernel,
        out_shape=jax.ShapeDtypeStruct((rows, width), BF16),
        in_specs=[VMEM] * 4,
        out_specs=VMEM,
        scratch_shapes=[
            pltpu.VMEM((pieces, rows, width // pieces), F32),
            pltpu.VMEM((pieces, rows, width // pieces), F32),
            pltpu.SemaphoreType.DMA((pieces,)),
            pltpu.SemaphoreType.DMA((pieces,)),
        ],
        compiler_params=params(1),
        name="output_projection",
    )(head_mixed, state_mixed, head_out_weight, state_out_weight)


def turn(value, same, swapped):
    return value * same + pltpu.roll(value, value.shape[1] // 2, 1) * swapped


def regroup(parts):
    block = lax.broadcasted_iota(jnp.int32, parts[0].shape, 1) // GROUP_CH
    parts = list(parts)
    for distance in (4, 2, 1):
        low = (block & distance) == 0
        amount = distance * GROUP_CH
        for i in range(len(parts)):
            if i & distance:
                continue
            first, second = parts[i], parts[i + distance]
            parts[i] = jnp.where(low, first, pltpu.roll(second, amount, 1))
            parts[i + distance] = jnp.where(low, pltpu.roll(first, LANES - amount, 1), second)
    return parts


def split(value):
    high = value.astype(BF16)
    return [high, (value - high.astype(F32)).astype(BF16)]


def local_kernel(
    state_ref, win_ref, x1g_ref, x3g_ref, x1d_ref, x3d_ref, inr_ref, ini_ref, outr_ref, outi_ref,
    zr_ref, zi_ref, et_ref, a16_ref, b16_ref, tail_ref, whole_ref, tile_ref,
    intra_ref, g_ref, pushed_ref, msg_ref, wide, uw,
):
    groups = zr_ref.shape[0]
    chunks = win_ref.shape[0] // groups
    span = win_ref.shape[1]
    per_tile = LANES // GROUP_CH
    for tile in range(groups // per_tile):
        wide[tile] = state_ref[:, pl.ds(tile * LANES, LANES)].astype(F32)
        for half in range(span // LANES):
            parts = regroup([
                wide[tile, pl.ds(half * per_tile + k, chunks, stride=CHUNK), :] for k in range(per_tile)
            ])
            for k in range(per_tile):
                rows = pl.ds((tile * per_tile + k) * chunks, chunks)
                columns = pl.ds(half * LANES, LANES)
                uw[rows, columns] = (parts[k] * win_ref[rows, columns]).astype(BF16)
    row = lax.broadcasted_iota(jnp.int32, (span, span), 0) // GROUP_CH
    column = lax.broadcasted_iota(jnp.int32, (span, span), 1) // GROUP_CH
    causal = row <= column
    batch = 4
    beside = lambda a, b: jnp.concatenate([a, b], axis=1)

    def table_of(g):
        one_row = pl.ds(g, 1)
        drive_in = beside(inr_ref[g], ini_ref[g])
        x2d = zr_ref[one_row, :] * drive_in + zi_ref[one_row, :] * beside(ini_ref[g], inr_ref[g])
        x4d = pltpu.roll(x2d, LANES // 2, 1)
        x2g = beside(outr_ref[g], outr_ref[g])
        x4g = beside(outi_ref[g], outi_ref[g])
        stack = lambda xs: jnp.concatenate([h for x in xs for h in split(x)], axis=0)
        return beside(
            stack([x1g_ref[g], x2g, x3g_ref[g], x4g]), stack([x1d_ref[g], x2d, x3d_ref[g], x4d])
        )

    def one(step, carry):
        ids = [step * batch + k for k in range(batch)]
        tall = [jnp.dot(et_ref[...], table_of(g), preferred_element_type=F32) for g in ids]
        both = [
            (x[:span] * x[span : 2 * span] + x[2 * span : 3 * span] * x[3 * span :]).astype(BF16)
            for x in tall
        ]
        out_side = [x[:, :LANES] for x in both]
        in_side = [x[:, LANES:] for x in both]
        for g, value in zip(ids, out_side):
            g_ref[g] = value
        table = [
            jnp.where(
                causal,
                lax.dot_general(a, b, (((1,), (1,)), ((), ())), preferred_element_type=F32),
                0.0,
            ).astype(BF16)
            for a, b in zip(in_side, out_side)
        ]
        for g, t, d in zip(ids, table, in_side):
            rows = pl.ds(pl.multiple_of(g * chunks, chunks), chunks)
            u = uw[rows, :]
            intra_ref[rows, :] = jnp.dot(u, t, preferred_element_type=F32)
            pushed_ref[rows, :] = jnp.dot(u, d, preferred_element_type=F32)
        return carry

    lax.fori_loop(0, groups // batch, one, 0)
    same, swapped = a16_ref[...], b16_ref[...]
    state = jnp.zeros((groups, pushed_ref.shape[1]), F32)
    for c in range(chunks):
        rows = pl.ds(c, groups, stride=chunks)
        local = tail_ref[rows, :] * turn(pushed_ref[rows, :], same, swapped)
        pushed_ref[rows, :] = local
        state = whole_ref[rows, :] * turn(state, same, swapped) + local
    msg_ref[:groups, :] = state
    msg_ref[groups:, :] = tile_ref[...]


def attend_block(block, first_device, query_ref, gate_ref, sink_ref, keys, values, head_ref):
    rows = pl.ds(block * WINDOW, WINDOW)
    band = pl.ds(block * WINDOW, 2 * WINDOW)
    query_index = lax.broadcasted_iota(jnp.int32, (WINDOW, 2 * WINDOW), 0)
    column = lax.broadcasted_iota(jnp.int32, (WINDOW, 2 * WINDOW), 1)
    distance = WINDOW + query_index - column
    allowed = (distance >= 0) & (distance < WINDOW)
    if block == 0:
        allowed = allowed & (column >= jnp.where(first_device, WINDOW, 0))
    group_size = Q_HEADS // KV_HEADS
    heads = query_ref.shape[1] // HEAD_DIM
    query, key, value = query_ref[rows, :], keys[band, :], values[band, :]
    gate = gate_ref[rows, :].astype(F32)
    results = []
    for head in range(heads):
        kv = head // group_size
        q = query[:, head * HEAD_DIM : (head + 1) * HEAD_DIM]
        k = key[:, kv * HEAD_DIM : (kv + 1) * HEAD_DIM]
        v = value[:, kv * HEAD_DIM : (kv + 1) * HEAD_DIM]
        scores = lax.dot_general(q, k, (((1,), (1,)), ((), ())), preferred_element_type=F32)
        scores = jnp.where(allowed, scores * HEAD_DIM ** (-0.5), NEG_FILL)
        sink = sink_ref[head]
        maxima = jnp.maximum(jnp.max(scores, axis=-1, keepdims=True), sink)
        exponent = jnp.exp(scores - maxima)
        totals = jnp.sum(exponent, axis=-1, keepdims=True) + jnp.exp(sink - maxima)
        weights = (exponent * (1.0 / totals)).astype(BF16)
        results.append(jnp.dot(weights, v, preferred_element_type=F32))
    attended = jnp.concatenate(results, axis=1)
    head_ref[rows, :] = (jax.nn.sigmoid(gate) * attended).astype(head_ref.dtype)


def carry_kernel(
    msg_ref, same_ref, swapped_ref, query_ref, key_ref, value_ref, gate_ref, sink_ref,
    carry_ref, head_ref, landed, keys, values, send_sem, recv_sem, halo_send, halo_recv,
):
    me = lax.axis_index("sp")
    count = lax.axis_size("sp")
    groups = carry_ref.shape[0]
    tok_rows = key_ref.shape[0]
    barrier = pltpu.get_barrier_semaphore()

    def greet(hop, x):
        pl.semaphore_signal(
            barrier, inc=1, device_id={"sp": lax.rem(me + hop, count)}, device_id_type=MESH
        )
        return x

    lax.fori_loop(1, count, greet, 0)
    pl.semaphore_wait(barrier, count - 1)

    def outgoing(target):
        return pltpu.make_async_remote_copy(
            src_ref=msg_ref,
            dst_ref=landed.at[me],
            send_sem=send_sem.at[target],
            recv_sem=recv_sem.at[me],
            device_id={"sp": target},
            device_id_type=MESH,
        )

    def incoming(source):
        return pltpu.make_async_remote_copy(
            src_ref=msg_ref,
            dst_ref=landed.at[source],
            send_sem=send_sem.at[source],
            recv_sem=recv_sem.at[source],
            device_id={"sp": source},
            device_id_type=MESH,
        )

    def halos(target):
        return [
            pltpu.make_async_remote_copy(
                src_ref=own.at[pl.ds(tok_rows - WINDOW, WINDOW)],
                dst_ref=band.at[pl.ds(0, WINDOW)],
                send_sem=halo_send.at[k],
                recv_sem=halo_recv.at[k],
                device_id={"sp": target},
                device_id_type=MESH,
            )
            for k, (own, band) in enumerate(((key_ref, keys), (value_ref, values)))
        ]

    @pl.when(me < count - 1)
    def _():
        for copy in halos(me + 1):
            copy.start()

    def send(target, x):
        outgoing(target).start()
        return x

    lax.fori_loop(me + 1, count, send, 0)
    own_rows = pl.ds(WINDOW, tok_rows)
    keys[own_rows, :] = key_ref[...]
    values[own_rows, :] = value_ref[...]

    @pl.when(me == 0)
    def _():
        keys[:WINDOW, :] = jnp.zeros((WINDOW, keys.shape[1]), keys.dtype)
        values[:WINDOW, :] = jnp.zeros((WINDOW, values.shape[1]), values.dtype)

    blocks = tok_rows // WINDOW
    for block in range(1, blocks):
        attend_block(block, me == 0, query_ref, gate_ref, sink_ref, keys, values, head_ref)

    @pl.when(me > 0)
    def _():
        for copy in halos(me):
            copy.wait_recv()

    attend_block(0, me == 0, query_ref, gate_ref, sink_ref, keys, values, head_ref)

    same, swapped = same_ref[...], swapped_ref[...]
    pick = lax.broadcasted_iota(jnp.int32, (groups, LANES), 0) == lax.broadcasted_iota(
        jnp.int32, (groups, LANES), 1
    )

    def absorb(source, state):
        incoming(source).wait_recv()
        shift_row = landed[source, pl.ds(groups, 1), :]
        total = jnp.sum(jnp.where(pick, shift_row, 0.0), axis=1, keepdims=True)
        return jnp.exp(total) * turn(state, same, swapped) + landed[source, pl.ds(0, groups), :]

    carry_ref[...] = lax.fori_loop(0, me, absorb, jnp.zeros(carry_ref.shape, F32))

    def drain(target, x):
        outgoing(target).wait_send()
        return x

    lax.fori_loop(me + 1, count, drain, 0)

    @pl.when(me < count - 1)
    def _():
        for copy in halos(me + 1):
            copy.wait_send()


def finish_kernel(
    carry_ref, pushed_ref, intra_ref, g_ref, wout_ref, a16_ref, b16_ref, head_ref, whole_ref,
    state_ref, gate_ref, skip_ref, mixed_ref, entry, grouped, rows_out,
):
    groups = g_ref.shape[0]
    chunks = pushed_ref.shape[0] // groups
    span = intra_ref.shape[1]
    per_tile = LANES // GROUP_CH
    same, swapped = a16_ref[...], b16_ref[...]
    state = carry_ref[...]
    for c in range(chunks):
        rows = pl.ds(c, groups, stride=chunks)
        entry[rows, :] = head_ref[rows, :] * state
        state = whole_ref[rows, :] * turn(state, same, swapped) + pushed_ref[rows, :]
    batch = 8

    def one(step, x):
        for k in range(batch):
            g = step * batch + k
            rows = pl.ds(pl.multiple_of(g * chunks, chunks), chunks)
            far = lax.dot_general(
                entry[rows, :].astype(BF16), g_ref[g], (((1,), (1,)), ((), ())),
                preferred_element_type=F32,
            )
            grouped[rows, :] = wout_ref[rows, :] * (intra_ref[rows, :] + far)
        return x

    lax.fori_loop(0, groups // batch, one, 0)
    for tile in range(groups // per_tile):
        lanes = pl.ds(tile * LANES, LANES)
        for half in range(span // LANES):
            columns = pl.ds(half * LANES, LANES)
            parts = regroup([
                grouped[pl.ds((tile * per_tile + k) * chunks, chunks), columns]
                for k in range(per_tile)
            ])
            for k in range(per_tile):
                rows_out[tile, pl.ds(half * per_tile + k, chunks, stride=CHUNK), :] = parts[k]
        recurrent = rows_out[tile] + skip_ref[:, lanes] * state_ref[:, lanes].astype(F32)
        gate = jax.nn.sigmoid(gate_ref[:, lanes].astype(F32))
        mixed_ref[:, lanes] = (gate * jax.nn.gelu(recurrent)).astype(mixed_ref.dtype)


def spread_matrix():
    span = CHUNK * GROUP_CH
    column = np.arange(span)
    by_step = (np.arange(CHUNK)[:, None] == column[None] // GROUP_CH).astype(np.float32)
    by_channel = (np.arange(GROUP_CH)[:, None] == column[None] % GROUP_CH).astype(np.float32)
    out = np.zeros((8 * CHUNK, 4 * span), np.float32)
    for kind in range(4):
        block = by_channel if kind % 2 else by_step
        for half in range(2):
            first = (2 * kind + half) * CHUNK
            out[first : first + CHUNK, kind * span : (kind + 1) * span] = block
    return out


def shift_matrix(states2):
    span = CHUNK * GROUP_CH
    step = np.arange(CHUNK)
    upto = (step[:, None] <= (np.arange(span) // GROUP_CH)[None]).astype(np.float32)
    ref = (step < CHUNK // 2).astype(np.float32)[:, None]
    relative = upto - ref
    return np.concatenate(
        [relative, np.repeat(ref, states2, 1), np.ones((CHUNK, states2), np.float32)], axis=1
    )


def tables(decay_real, decay_frequency, log_step, chunks):
    decay_real = jnp.concatenate([decay_real, decay_real], axis=1)
    decay_frequency = jnp.concatenate([decay_frequency, decay_frequency], axis=1)
    width = decay_real.shape[1]
    low = jnp.arange(width) < width // 2
    stepsize = jnp.exp(log_step)[:, None]
    log_magnitude = decay_real * stepsize
    rotation = decay_frequency * stepsize
    magnitude = jnp.exp(log_magnitude)
    base_real = magnitude * jnp.cos(rotation)
    base_imag = magnitude * jnp.sin(rotation)
    denominator = decay_real * decay_real + decay_frequency * decay_frequency
    less_real = base_real - 1.0
    zoh_real = (less_real * decay_real + base_imag * decay_frequency) / denominator
    zoh_imag = (base_imag * decay_real - less_real * decay_frequency) / denominator
    counter = jnp.arange(1, CHUNK + 1, dtype=F32)[None, :, None]
    angle = counter * rotation[:, None, :]
    cosine, sine = jnp.cos(angle), jnp.sin(angle)
    grow = jnp.exp(counter * log_magnitude[:, None, :])
    shrink = jnp.exp(-counter * log_magnitude[:, None, :])
    power_real, power_imag = grow * cosine, grow * sine
    x1g = jnp.where(low, power_real, -power_imag)
    x3g = jnp.where(low, -power_imag, -power_real)
    x1d = shrink * cosine
    x3d = jnp.where(low, shrink * sine, -(shrink * sine))
    last_real, last_imag = power_real[:, -1], power_imag[:, -1]
    all_real, all_imag = last_real, last_imag
    for _ in range(chunks - 1):
        all_real, all_imag = (
            all_real * last_real - all_imag * last_imag,
            all_real * last_imag + all_imag * last_real,
        )
    sign = lambda value: jnp.where(low, -value, value)
    return (
        (x1g, x3g, x1d, x3d, zoh_real, sign(zoh_imag)),
        (last_real, sign(last_imag)),
        (all_real, sign(all_imag)),
    )


def on_device(
    hidden,
    query_weight,
    key_weight,
    value_weight,
    head_gate_weight,
    state_in_weight,
    state_gate_weight,
    sink_logit,
    decay_real,
    decay_frequency,
    log_step,
    input_real,
    input_imaginary,
    output_real,
    output_imaginary,
    skip_weight,
    decay_shift,
    head_out_weight,
    state_out_weight,
):
    portion = gather_hidden(hidden)
    state_input, query, key, value, head_gate, state_gate = (
        jnp.dot(portion, weight, preferred_element_type=F32).astype(BF16)
        for weight in (
            state_in_weight, query_weight, key_weight, value_weight, head_gate_weight,
            state_gate_weight,
        )
    )
    tok_rows = hidden.shape[0]
    groups, states = decay_real.shape
    chunks = tok_rows // CHUNK
    span = CHUNK * GROUP_CH
    states2 = 2 * states
    rows = groups * chunks
    prepared, (a16, b16), (a_all, b_all) = tables(decay_real, decay_frequency, log_step, chunks)
    x1g, x3g, x1d, x3d, zoh_real, zoh_imag = prepared
    sums = jnp.dot(
        decay_shift.reshape(rows, CHUNK), jnp.asarray(shift_matrix(states2)),
        precision=lax.Precision.HIGHEST,
    )
    relative = sums[:, :span]
    head = jnp.exp(sums[:, span : span + states2])
    whole_log = sums[:, span + states2 :]
    whole = jnp.exp(whole_log)
    tail = jnp.exp(whole_log - sums[:, span : span + states2])
    weight_out, weight_in = jnp.exp(relative), jnp.exp(-relative)
    tile = jnp.pad(jnp.sum(decay_shift, axis=1)[None], ((0, 7), (0, LANES - groups)))
    intra, g_out, pushed, message = pl.pallas_call(
        local_kernel,
        out_shape=(
            jax.ShapeDtypeStruct((rows, span), F32),
            jax.ShapeDtypeStruct((groups, span, states2), BF16),
            jax.ShapeDtypeStruct((rows, states2), F32),
            jax.ShapeDtypeStruct((groups + 8, LANES), F32),
        ),
        in_specs=[VMEM] * 18,
        out_specs=(VMEM,) * 4,
        scratch_shapes=[
            pltpu.VMEM((groups * GROUP_CH // LANES, tok_rows, LANES), F32),
            pltpu.VMEM((rows, span), BF16),
        ],
        compiler_params=params(),
        name="state_local",
    )(
        state_input, weight_in, x1g, x3g, x1d, x3d, input_real.transpose(0, 2, 1),
        input_imaginary.transpose(0, 2, 1), output_real, output_imaginary, zoh_real, zoh_imag,
        jnp.asarray(spread_matrix().T, BF16), a16, b16, tail, whole, tile,
    )
    count = lax.axis_size("sp")
    carry, head_mixed = pl.pallas_call(
        carry_kernel,
        out_shape=(
            jax.ShapeDtypeStruct((groups, states2), F32),
            jax.ShapeDtypeStruct(query.shape, BF16),
        ),
        in_specs=[VMEM] * 7 + [pl.BlockSpec(memory_space=pltpu.SMEM)],
        out_specs=(VMEM, VMEM),
        scratch_shapes=[
            pltpu.VMEM((count, groups + 8, LANES), F32),
            pltpu.VMEM((WINDOW + tok_rows, key.shape[1]), BF16),
            pltpu.VMEM((WINDOW + tok_rows, key.shape[1]), BF16),
            pltpu.SemaphoreType.DMA((count,)),
            pltpu.SemaphoreType.DMA((count,)),
            pltpu.SemaphoreType.DMA((2,)),
            pltpu.SemaphoreType.DMA((2,)),
        ],
        compiler_params=params(2),
        name="carry_and_attention",
    )(message, a_all, b_all, query, key, value, head_gate, sink_logit)
    state_mixed = pl.pallas_call(
        finish_kernel,
        out_shape=jax.ShapeDtypeStruct((tok_rows, groups * GROUP_CH), BF16),
        in_specs=[VMEM] * 12,
        out_specs=VMEM,
        scratch_shapes=[
            pltpu.VMEM((rows, states2), F32),
            pltpu.VMEM((rows, span), F32),
            pltpu.VMEM((groups * GROUP_CH // LANES, tok_rows, LANES), F32),
        ],
        compiler_params=params(),
        name="state_finish",
    )(
        carry, pushed, intra, g_out, weight_out, a16, b16, head, whole, state_input, state_gate,
        skip_weight.reshape(1, -1),
    )
    return project_out(head_mixed, state_mixed, head_out_weight, state_out_weight)


def solution(mesh):
    in_specs = (
        P("sp", "tp"),
        P(None, "tp"),
        P(None, "tp"),
        P(None, "tp"),
        P(None, "tp"),
        P(None, "tp"),
        P(None, "tp"),
        P("tp"),
        P("tp", None),
        P("tp", None),
        P("tp"),
        P("tp", None, None),
        P("tp", None, None),
        P("tp", None, None),
        P("tp", None, None),
        P("tp", None),
        P("tp", "sp"),
        P("tp", None),
        P("tp", None),
    )
    out_specs = P("sp", "tp")
    return jax.shard_map(
        on_device, mesh=mesh, in_specs=in_specs, out_specs=out_specs, check_vma=False
    )
```

profile of v0, /device:TPU:25, one launch (start us, length us, event | category | flops | bytes accessed | tf_op | source)
XLA Modules:
  0.0 76.3 jit_solution(12693307690127511063)
XLA Ops:
  0.0 0.0 copy-start
  0.0 0.8 %exp.28 = f32[32]{0:T(128)S(1)} exponential(f32[32]{0:T(128)} %param.31) | non-fusion elementwise | bytes 256 | tf_op jit(solution)/shard_map/exp | solution.py:432
  0.8 1.6 %negate_select_fusion.5 = (f32[32,128]{1,0:T(8,128)}, f32[32,128]{1,0:T(8,128)}, f32[32,128]{1,0:T(8,128)S(1)}, f32[32,128]{1,0:T(8,128)S(1)}) fusion(f32[32,64]{1,0:T(8,128)} %param.30, f32[32,64]{1,0:T(8,128)} %param.29, pred[128]{0:T(512)(128)(4,1)S(1)} %iota_compare_fusion, f32[32]{0:T(128)S(1)} %exp.28), kind=kLoop, calls=%fused_computation.25 | loop fusion | flops 81920 | bytes 82176 | tf_op jit(solution)/shard_map/jit(_where)/select_n | solution.py:459
  2.4 1.1 %negate_select_fusion = (f32[32,16,128]{2,0,1:T(8,128)S(1)}, f32[32,16,128]{2,0,1:T(8,128)S(1)}, f32[32,16,128]{2,0,1:T(8,128)S(1)}, f32[32,16,128]{2,0,1:T(8,12...) fusion(f32[16]{0:T(128)S(1)} %get-tuple-element.36, f32[32,128]{1,0:T(8,128)S(1)} %get-tuple-element.34, ...), kind=kLoop, calls=%fused_computation.9 | loop fusion | flops 851968 | bytes 1605888 | tf_op jit(solution)/shard_map/jit(_where)/select_n | solution.py:451
  3.5 0.7 negate_select_fusion.3
  4.2 0.6 slice_bitcast_fusion.1.a16_ref
  4.8 0.9 %copy.29.x1g_ref = f32[32,16,128]{2,1,0:T(8,128)} copy(f32[32,16,128]{2,0,1:T(8,128)S(1)} %get-tuple-element.26) | data formatting | bytes 524288 | tf_op jit(solution)/shard_map/jit(_where)/select_n | solution.py:448
  5.7 0.9 %copy.30.x3g_ref = f32[32,16,128]{2,1,0:T(8,128)} copy(f32[32,16,128]{2,0,1:T(8,128)S(1)} %get-tuple-element.27) | data formatting | bytes 524288 | tf_op jit(solution)/shard_map/jit(_where)/select_n | solution.py:449
  6.5 0.9 %copy.31.x1d_ref = f32[32,16,128]{2,1,0:T(8,128)} copy(f32[32,16,128]{2,0,1:T(8,128)S(1)} %get-tuple-element.28) | data formatting | bytes 524288 | tf_op jit(solution)/shard_map/mul | solution.py:450
  7.4 0.9 %copy.32.x3d_ref = f32[32,16,128]{2,1,0:T(8,128)} copy(f32[32,16,128]{2,0,1:T(8,128)S(1)} %get-tuple-element.25) | data formatting | bytes 524288 | tf_op jit(solution)/shard_map/jit(_where)/select_n | solution.py:451
  8.3 4.2 %hidden_exchange.1 = bf16[256,2048]{1,0:T(8,128)(2,1)} custom-call(bf16[256,1024]{1,0:T(8,128)(2,1)} %own_ref.1), custom_call_target="tpu_custom_call" | custom-call | tf_op jit(solution)/shard_map/hidden_exchange/pallas_call | solution.py:52
  12.5 0.0 copy-start.4
  12.5 0.0 copy-start.5
  12.5 2.6 %convolution_convert_fusion.3.state_ref = bf16[256,512]{1,0:T(8,128)(2,1)} fusion(bf16[256,2048]{1,0:T(8,128)(2,1)} %hidden_exchange.1, bf16[2048,512]{1,0:T(8,128)(2,1)S(1)} %copy-done), kind=kOutput, calls=%fused_computation.4 | convolution fusion | flops 537001984 | bytes 3407872 | tf_op jit(solution)/shard_map/dot_general | solution.py:490
  15.2 0.1 reshape.64
  15.3 1.0 %convolution_bitcast_fusion = f32[512,512]{1,0:T(8,128)S(1)} fusion(f32[16,512]{1,0:T(8,128)S(1)} %copy-done.5, f32[512,16]{1,0:T(8,128)S(1)} %reshape.64), kind=kOutput, calls=%fused_computation | convolution fusion | flops 50331648 | bytes 1114112 | tf_op jit(solution)/shard_map/dot_general | solution.py:504
  16.3 1.0 %slice_exponential_fusion.1 = (f32[512,128]{1,0:T(8,128)}, f32[512,128]{1,0:T(8,128)}, f32[512,128]{1,0:T(8,128)}) fusion(f32[512,512]{1,0:T(8,128)S(1)} %convolution_bitcast_fusion), kind=kLoop, calls=%fused_computation.20 | loop fusion | flops 65536 | bytes 1310720 | tf_op jit(solution)/shard_map/exp | solution.py:509
  17.2 1.1 %slice_exponential_fusion = (f32[512,256]{1,0:T(8,128)}, f32[512,256]{1,0:T(8,128)}) fusion(f32[512,512]{1,0:T(8,128)S(1)} %convolution_bitcast_fusion), kind=kLoop, calls=%fused_computation.8 | loop fusion | flops 131072 | bytes 1572864 | tf_op jit(solution)/shard_map/exp | solution.py:513
  18.3 0.1 reduce_sum.9
  18.5 0.6 pad.4.tile_ref
  19.1 14.2 %state_local.1 = (f32[512,256]{1,0:T(8,128)}, bf16[32,256,128]{2,1,0:T(8,128)(2,1)}, f32[512,128]{1,0:T(8,128)}, f32[40,128]{1,0:T(8,128)}) custom-call(bf16[256,512]{1,0:T(8,128)(2,1)} %convolution_convert_fusion.3.state_ref, f32[512,256]{1,0:T(8,128)} %get-tuple-element.21.win_ref, f32[32,16,128]{2,1,0:T(8,128)} %copy.29.x1g_ref, ...), custom_call_target="tpu_custom_call" | custom-call | tf_op jit(solution)/shard_map/state_local/pallas_call | solution.py:515
  33.3 3.1 %convolution_convert_fusion.1.gate_ref = bf16[256,512]{1,0:T(8,128)(2,1)} fusion(bf16[256,2048]{1,0:T(8,128)(2,1)S(1)} %copy-done.1, bf16[2048,512]{1,0:T(8,128)(2,1)} %param.25), kind=kOutput, calls=%fused_computation.2 | convolution fusion | flops 537001984 | bytes 3407872 | tf_op jit(solution)/shard_map/dot_general | solution.py:490
  36.4 1.4 %convolution_convert_fusion.2.query_ref = bf16[256,512]{1,0:T(8,128)(2,1)} fusion(bf16[256,2048]{1,0:T(8,128)(2,1)S(1)} %copy-done.1, bf16[2048,512]{1,0:T(8,128)(2,1)S(1)} %copy-done.7), kind=kOutput, calls=%fused_computation.3 | convolution fusion | flops 537001984 | bytes 3407872 | tf_op jit(solution)/shard_map/dot_general | solution.py:490
  37.8 1.1 %convolution_convert_fusion.4.value_ref = bf16[256,256]{1,0:T(8,128)(2,1)} fusion(bf16[256,2048]{1,0:T(8,128)(2,1)S(1)} %copy-done.1, bf16[2048,256]{1,0:T(8,128)(2,1)S(1)} %copy-done.2), kind=kOutput, calls=%fused_computation.5 | convolution fusion | flops 268500992 | bytes 2228224 | tf_op jit(solution)/shard_map/dot_general | solution.py:490
  38.9 1.1 %convolution_convert_fusion.5.key_ref = bf16[256,256]{1,0:T(8,128)(2,1)} fusion(bf16[256,2048]{1,0:T(8,128)(2,1)S(1)} %copy-done.1, bf16[2048,256]{1,0:T(8,128)(2,1)S(1)} %copy-done.3), kind=kOutput, calls=%fused_computation.6 | convolution fusion | flops 268500992 | bytes 2228224 | tf_op jit(solution)/shard_map/dot_general | solution.py:490
  40.0 15.6 %carry_and_attention.1 = (f32[32,128]{1,0:T(8,128)}, bf16[256,512]{1,0:T(8,128)(2,1)}) custom-call(f32[40,128]{1,0:T(8,128)} %get-tuple-element.11.msg_ref, f32[32,128]{1,0:T(8,128)} %get-tuple-element.23.same_ref, f32[32,128]{1,0:T(8,128)} %get-tuple-element.22.swapped_ref, bf16[256,512]{1,0:T(8,128)(2,1)} %convolution_convert_fusion.2.query_ref, ...), custom_call_target="tpu_custom_call" | custom-call | tf_op jit(solution)/shard_map/carry_and_attention/pallas_call | solution.py:537
  55.6 3.0 %convolution_convert_fusion.gate_ref = bf16[256,512]{1,0:T(8,128)(2,1)} fusion(bf16[256,2048]{1,0:T(8,128)(2,1)S(1)} %copy-done.1, bf16[2048,512]{1,0:T(8,128)(2,1)} %param.27), kind=kOutput, calls=%fused_computation.1 | convolution fusion | flops 537001984 | bytes 3407872 | tf_op jit(solution)/shard_map/dot_general | solution.py:490
  58.6 0.1 copy.33
  58.6 0.7 reshape.65.skip_ref
  59.3 6.2 %state_finish.1.state_ref = bf16[256,512]{1,0:T(8,128)(2,1)} custom-call(f32[32,128]{1,0:T(8,128)} %get-tuple-element.13.carry_ref, f32[512,128]{1,0:T(8,128)} %get-tuple-element.14.pushed_ref, f32[512,256]{1,0:T(8,128)} %get-tuple-element.15.intra_ref, bf16[32,256,128]{2,1,0:T(8,128)(2,1)} %get-tuple-element.16.g_ref, ...), custom_call_target="tpu_custom_call" | custom-call | tf_op jit(solution)/shard_map/state_finish/pallas_call | solution.py:557
  65.5 9.0 %output_projection.1 = bf16[256,1024]{1,0:T(8,128)(2,1)} custom-call(bf16[256,512]{1,0:T(8,128)(2,1)} %get-tuple-element.12.head_ref, bf16[256,512]{1,0:T(8,128)(2,1)} %state_finish.1.state_ref, bf16[512,2048]{1,0:T(8,128)(2,1)} %how_ref.1, bf16[512,2048]{1,0:T(8,128)(2,1)} %sow_ref.1), custom_call_target="tpu_custom_call" | custom-call | tf_op jit(solution)/shard_map/output_projection/pallas_call | solution.py:106
  74.5 1.9 %copy.36 = bf16[256,1024]{1,0:T(8,128)(2,1)} copy(bf16[256,1024]{1,0:T(8,128)(2,1)} %output_projection.1) | data formatting | bytes 1048576
  (15 shorter events, 0.0 us)
Async XLA Ops:
  0.0 12.5 %copy-start = (bf16[2048,512]{1,0:T(8,128)(2,1)S(1)}, bf16[2048,512]{1,0:T(8,128)(2,1)}, u32[]{:S(2)}) copy-start(bf16[2048,512]{1,0:T(8,128)(2,1)} %param.26) | copy-start | bytes 6291460
  12.5 2.7 %copy-start.4 = (f32[32,256]{1,0:T(8,128)S(1)}, f32[32,256]{1,0:T(8,128)}, u32[]{:S(2)}) copy-start(f32[32,256]{1,0:T(8,128)} %param.37) | copy-start | bytes 98308
  12.5 2.8 %copy-start.5 = (f32[16,512]{1,0:T(8,128)S(1)}, f32[16,512]{1,0:T(8,128)}, u32[]{:S(2)}) copy-start(f32[16,512]{1,0:T(8,128)} %constant.15.clone) | copy-start | bytes 98308
  18.3 14.9 %copy-start.1 = (bf16[256,2048]{1,0:T(8,128)(2,1)S(1)}, bf16[256,2048]{1,0:T(8,128)(2,1)}, u32[]{:S(2)}) copy-start(bf16[256,2048]{1,0:T(8,128)(2,1)} %hidden_exchange.1) | copy-start | bytes 3145732
  33.3 3.2 %copy-start.7 = (bf16[2048,512]{1,0:T(8,128)(2,1)S(1)}, bf16[2048,512]{1,0:T(8,128)(2,1)}, u32[]{:S(2)}) copy-start(bf16[2048,512]{1,0:T(8,128)(2,1)} %param.22) | copy-start | bytes 6291460
  36.4 1.4 %copy-start.2 = (bf16[2048,256]{1,0:T(8,128)(2,1)S(1)}, bf16[2048,256]{1,0:T(8,128)(2,1)}, u32[]{:S(2)}) copy-start(bf16[2048,256]{1,0:T(8,128)(2,1)} %param.24) | copy-start | bytes 3145732
  36.4 2.5 %copy-start.3 = (bf16[2048,256]{1,0:T(8,128)(2,1)S(1)}, bf16[2048,256]{1,0:T(8,128)(2,1)}, u32[]{:S(2)}) copy-start(bf16[2048,256]{1,0:T(8,128)(2,1)} %param.23) | copy-start | bytes 3145732
  40.0 18.6 %copy-start.6 = (f32[32,16]{0,1:T(8,128)S(1)}, f32[32,16]{0,1:T(8,128)}, u32[]{:S(2)}) copy-start(f32[32,16]{0,1:T(8,128)} %param.36) | copy-start | bytes 6148
where the time goes:
time: 76.7 us; the launch traced here: 76.3 us
  Pallas kernels  49.2 us (64%)
  matrix products  13.3 us (17%)
  local copies, waits for them, and re-layouts  8.23 us (11%)
  other arithmetic  5.54 us (7%)
    pallas_call x1, Pallas kernels, on_device(): pl.pallas_call(carry_kernel, out_shape=(jax.ShapeDtypeStruct((groups, sta...  15.6 us
    pallas_call x1, Pallas kernels, on_device(): pl.pallas_call(local_kernel, out_shape=(jax.ShapeDtypeStruct((rows, span)...  14.2 us
    dot_general x6, matrix products, on_device(): jnp.dot(portion, weight, preferred_element_type=F32).astype(BF16)  12.3 us
    pallas_call x1, Pallas kernels, project_out(): pl.pallas_call(output_kernel, out_shape=jax.ShapeDtypeStruct((rows, width...  8.96 us
    pallas_call x1, Pallas kernels, on_device(): pl.pallas_call(finish_kernel, out_shape=jax.ShapeDtypeStruct((tok_rows, g...  6.2 us
    pallas_call x1, Pallas kernels, gather_hidden(): pl.pallas_call(hidden_kernel, out_shape=jax.ShapeDtypeStruct((rows, 2 * w...  4.24 us
    select_n x2, other arithmetic, tables(): sign = lambda value: jnp.where(low, -value, value)  2.23 us
    unnamed x18, local copies, waits for them, and re-layouts  1.98 us

commit v1 on v0

v1 whole, which is shorter than its diff:
```python
import jax
import jax.numpy as jnp
import numpy as np
from jax import lax
from jax.experimental import pallas as pl
from jax.experimental.pallas import tpu as pltpu
from jax.sharding import PartitionSpec as P

HEAD_DIM = 64
Q_HEADS = 16
KV_HEADS = 8
GROUP_CH = 16
WINDOW = 128
LANES = 128
SEGS = 8
TILE = 256

NEG_FILL = -1e30
MESH = pl.DeviceIdType.MESH
ANY = pl.BlockSpec(memory_space=pl.ANY)
VMEM = pl.BlockSpec(memory_space=pltpu.VMEM)
SMEM = pl.BlockSpec(memory_space=pltpu.SMEM)
BF16 = jnp.bfloat16
F32 = jnp.float32
NT = (((1,), (1,)), ((), ()))


def split(value, pieces):
    out = []
    for _ in range(pieces):
        high = value.astype(BF16)
        out.append(high)
        value = value - high.astype(F32)
    return out


def ndot(a, b):
    return jnp.dot(a, b, preferred_element_type=F32)


def ntdot(a, b):
    return lax.dot_general(a, b, NT, preferred_element_type=F32)


def cmul(ar, ai, br, bi):
    return ar * br - ai * bi, ar * bi + ai * br


REF, FIN, PRE, ONE, TWO, FOUR, ALL = range(7)


def constants(rows, groups, states):
    length = rows // SEGS
    time = np.arange(rows)
    seg, pos = time // length, time % length
    order = (time % SEGS) * length + time // SEGS
    permute = (order[:, None] == time[None]).astype(np.float32)
    same = seg[order][:, None] == seg[None]
    upto = (order[:, None] >= time[None]).astype(np.float32)
    first = (pos < length // 2).astype(np.float32)[None]
    running = same * (upto - first)
    k = np.arange(SEGS)[:, None]
    here = seg[None] == k
    sums = np.concatenate(
        [
            here * first,
            here * (1 - first),
            seg[None] < k,
            here,
            (seg[None] <= k) & (seg[None] > k - 2),
            (seg[None] <= k) & (seg[None] > k - 4),
            np.ones((SEGS, rows)),
        ],
        axis=0,
    ).astype(np.float32)
    column = np.arange(groups * GROUP_CH) // GROUP_CH
    spread = (np.arange(groups)[:, None] == column[None]).astype(np.float32)
    lane = np.arange(groups * states) // states
    widen = (np.arange(groups)[:, None] == lane[None]).astype(np.float32)
    make = lambda x: jnp.asarray(x, BF16)
    return (
        make(permute), make(permute.T), make(running), make(sums),
        make(np.concatenate([spread, spread], axis=0)), make(np.concatenate([widen] * 3, axis=0)),
    )


def per_pair(row, pairs):
    spots = row.shape[1]
    wide = jnp.broadcast_to(row, (pairs, spots))
    r = lax.broadcasted_iota(jnp.int32, (pairs, spots), 0)
    c = lax.broadcasted_iota(jnp.int32, (pairs, spots), 1)
    even = jnp.sum(jnp.where(c == 2 * r, wide, 0.0), axis=1, keepdims=True)
    odd = jnp.sum(jnp.where(c == 2 * r + 1, wide, 0.0), axis=1, keepdims=True)
    low = lax.broadcasted_iota(jnp.int32, (pairs, LANES), 1) < LANES // 2
    return jnp.where(low, even, odd)


def layer_kernel(
    hidden_ref, wq_ref, wk_ref, wv_ref, wg_ref, wsi_ref, wsg_ref, sink_ref, dr_in, df_in, ls_in, ir_in, ii_in,
    or_in, oi_in, skip_in, shift_in, how_ref, sow_ref, permute_in, back_in, running_in, sums_in, spread_in, widen_in,
    out_ref,
    x, w, how, sow, dr, df, ls, ir, ii, orr, oi, skip, shift, permute, back, running, sums, spread, widen,
    drive, readout, pushed, states_ref, u_ref, gate_ref, win, wout, base, power, table, zoh, entry, init,
    proj, keys, values, mixed, head, near, far, acc_me, acc_other, away, landed,
    in_sem, w_sem, x_send, x_recv, near_send, near_recv, far_send, far_recv, halo_send, halo_recv, out_send, out_recv,
):
    tp = lax.axis_index("tp")
    other = 1 - tp
    me = lax.axis_index("sp")
    count = lax.axis_size("sp")
    inner, outer = near.shape[0], far.shape[0]
    mine, plane = lax.rem(me, inner), lax.div(me, inner)
    rows, half_width = hidden_ref.shape
    pairs = drive.shape[0]
    groups = 2 * pairs
    length = rows // SEGS
    per_tile = LANES // GROUP_CH
    tiles = groups // per_tile
    pairs_tile = per_tile // 2

    local = pltpu.make_async_copy
    own_x = local(hidden_ref, x.at[tp], in_sem.at[0])
    small = [
        local(src, dst, in_sem.at[1 + i])
        for i, (src, dst) in enumerate((
            (dr_in, dr), (df_in, df), (ls_in, ls), (shift_in, shift), (running_in, running), (sums_in, sums),
            (spread_in, spread), (widen_in, widen), (ir_in, ir), (ii_in, ii), (or_in, orr), (oi_in, oi),
            (skip_in, skip), (permute_in, permute), (back_in, back), (how_ref, how), (sow_ref, sow),
        ))
    ]
    columns = []
    for ref in (wsi_ref, wk_ref, wv_ref, wq_ref, wg_ref, wsg_ref):
        for c in range(ref.shape[1] // TILE):
            columns.append(ref.at[:, pl.ds(c * TILE, TILE)])
    weights = [local(src, w.at[i], w_sem.at[i]) for i, src in enumerate(columns)]
    own_x.start()
    for copy in small[:-2]:
        copy.start()
    for copy in weights:
        copy.start()
    for copy in small[-2:]:
        copy.start()

    barrier = pltpu.get_barrier_semaphore()
    pl.semaphore_signal(barrier, inc=1, device_id={"tp": other}, device_id_type=MESH)
    for hop in range(1, inner):
        target = plane * inner + lax.rem(mine + hop, inner)
        pl.semaphore_signal(barrier, inc=1, device_id={"sp": target}, device_id_type=MESH)
    for hop in range(1, outer):
        target = lax.rem(plane + hop, outer) * inner + mine
        pl.semaphore_signal(barrier, inc=1, device_id={"sp": target}, device_id_type=MESH)
    for step in (1, count - 1):
        target = lax.rem(me + step, count)
        pl.semaphore_signal(barrier, inc=1, device_id={"sp": target}, device_id_type=MESH)

    zero = jnp.zeros((LANES, TILE), BF16)
    for q in range(pairs):
        drive[q] = zero
        readout[q] = zero
    for copy in small[:3]:
        copy.wait()
    two = lambda ref: jnp.concatenate(
        [ref[pl.ds(0, pairs, stride=2), :], ref[pl.ds(1, pairs, stride=2), :]], axis=1
    )
    decay, frequency = two(dr), two(df)
    stepsize = jnp.exp(per_pair(ls[...], pairs))
    magnitude = jnp.exp(decay * stepsize)
    rotation = frequency * stepsize
    base_r, base_i = magnitude * jnp.cos(rotation), magnitude * jnp.sin(rotation)
    denominator = decay * decay + frequency * frequency
    less = base_r - 1.0
    zoh[0] = (less * decay + base_i * frequency) / denominator
    zoh[1] = (base_i * decay - less * frequency) / denominator
    base[0], base[1] = base_r, base_i
    power_r, power_i = base_r, base_i
    for _ in range(length.bit_length() - 1):
        power_r, power_i = cmul(power_r, power_i, power_r, power_i)
    for d in range(3):
        base[2 + 2 * d], base[3 + 2 * d] = power_r, power_i
        power_r, power_i = cmul(power_r, power_i, power_r, power_i)
    block_r, block_i = power_r, power_i
    run_r, run_i = jnp.ones_like(base_r), jnp.zeros_like(base_r)
    for k in range(SEGS):
        spot = pl.ds(k, pairs, stride=SEGS)
        power[0, spot, :] = run_r
        power[1, spot, :] = run_i
        run_r, run_i = cmul(run_r, run_i, base[2], base[3])

    for copy in small[3:8]:
        copy.wait()
    shifts = split(shift[...], 3)
    relative = sum(ntdot(running[...], piece) for piece in shifts)
    grown = jnp.concatenate(split(jnp.exp(-relative), 2), axis=1)
    win[...] = ndot(grown, spread[...])
    shrunk = jnp.concatenate(split(jnp.exp(relative), 2), axis=1)
    wout[...] = ndot(shrunk, spread[...])
    totals = sum(ntdot(sums[...], piece) for piece in shifts)
    message_shift = totals[ALL * SEGS : (ALL + 1) * SEGS]
    scales = jnp.concatenate(split(jnp.exp(totals), 3), axis=1)
    table[...] = ndot(scales, widen[...])

    for copy in small[8:12]:
        copy.wait()
    row_low = lax.broadcasted_iota(jnp.int32, (2 * GROUP_CH, LANES), 0) < GROUP_CH
    lane_low = lax.broadcasted_iota(jnp.int32, (2 * GROUP_CH, LANES), 1) < LANES // 2
    own_lane = row_low == lane_low
    for q in range(pairs):
        pick = lambda ref: jnp.concatenate([
            jnp.concatenate([ref[2 * q], ref[2 * q]], axis=1),
            jnp.concatenate([ref[2 * q + 1], ref[2 * q + 1]], axis=1),
        ], axis=0)
        spot = pl.ds((q % pairs_tile) * 2 * GROUP_CH, 2 * GROUP_CH)
        in_r, in_i = pick(ir), pick(ii)
        z_r, z_i = zoh[0, q : q + 1, :], zoh[1, q : q + 1, :]
        d_r, d_i = cmul(z_r, z_i, in_r, in_i)
        drive[q, spot, :] = jnp.concatenate(
            [jnp.where(own_lane, d_r, 0.0), jnp.where(own_lane, d_i, 0.0)], axis=1
        ).astype(BF16)
        readout[q, spot, :] = jnp.concatenate(
            [jnp.where(own_lane, pick(orr), 0.0), jnp.where(own_lane, -pick(oi), 0.0)], axis=1
        ).astype(BF16)

    own_x.wait()
    pl.semaphore_wait(barrier, inner + outer + 1)
    swap = pltpu.make_async_remote_copy(
        src_ref=x.at[tp], dst_ref=x.at[tp], send_sem=x_send, recv_sem=x_recv,
        device_id={"tp": other}, device_id_type=MESH,
    )
    swap.start()
    small[12].wait()
    lanes_of = lax.broadcasted_iota(jnp.int32, (GROUP_CH, groups * GROUP_CH), 1) % GROUP_CH
    channel = lax.broadcasted_iota(jnp.int32, (GROUP_CH, groups * GROUP_CH), 0)
    skips = sum(ndot(piece, spread[:groups, :]) for piece in split(skip[...], 3))
    skip_row = jnp.sum(jnp.where(lanes_of == channel, skips, 0.0), axis=0, keepdims=True)
    small[13].wait()
    small[14].wait()
    swap.wait()

    def project(n):
        weights[n].wait()
        return (ndot(x[0], w[n, :half_width, :]) + ndot(x[1], w[n, half_width:, :])).astype(BF16)

    SI, KEY, VALUE = 0, 2, 3
    QUERY, GATE, SGATE = 4, 6, 8

    for c in range(2):
        lanes = pl.ds(c * TILE, TILE)
        u = ndot(permute[...], project(SI + c))
        u_ref[:, lanes] = u.astype(BF16)
        weighted = (u * win[:, lanes]).astype(BF16)
        for t in range(TILE // LANES):
            tile = c * (TILE // LANES) + t
            part = weighted[:, t * LANES : (t + 1) * LANES]
            for i in range(pairs_tile):
                q = tile * pairs_tile + i
                pushed[q] = ndot(part, drive[q])

    bunch = 8

    def wide(ref, index, q):
        return jnp.broadcast_to(ref[index, q : q + 1, :], (SEGS, LANES))

    def scan(first, start, keep):
        br = [wide(base, 0, first + i) for i in range(bunch)]
        bi = [wide(base, 1, first + i) for i in range(bunch)]

        def steps(jj, carry):
            carry = list(carry)
            kept = [[] for _ in range(2 * bunch)]
            for sub in range(2):
                spot = pl.ds(pl.multiple_of((2 * jj + sub) * SEGS, SEGS), SEGS)
                for i in range(bunch):
                    r, m = carry[2 * i], carry[2 * i + 1]
                    p = pushed[first + i, spot, :]
                    new_r = br[i] * r - bi[i] * m + p[:, :LANES]
                    new_m = br[i] * m + bi[i] * r + p[:, LANES:]
                    carry[2 * i], carry[2 * i + 1] = new_r, new_m
                    kept[2 * i].append(new_r)
                    kept[2 * i + 1].append(new_m)
            if keep:
                spot = pl.ds(pl.multiple_of(jj * 2 * SEGS, 2 * SEGS), 2 * SEGS)
                for i in range(bunch):
                    for part in range(2):
                        value = jnp.concatenate(kept[2 * i + part], axis=0).astype(BF16)
                        states_ref[first + i, spot, pl.ds(part * LANES, LANES)] = value
            return tuple(carry)

        return lax.fori_loop(0, length // 2, steps, tuple(start), unroll=2)

    def row(kind, q):
        return table[kind * SEGS : (kind + 1) * SEGS, q * LANES : (q + 1) * LANES]

    sub = lax.broadcasted_iota(jnp.int32, (SEGS, LANES), 0)
    near_me = near.at[mine]
    near_me[2 * pairs :, :] = jnp.concatenate(
        [message_shift, jnp.zeros((SEGS, LANES - groups), F32)], axis=1
    )
    for first in range(0, pairs, bunch):
        ends = scan(first, [jnp.zeros((SEGS, LANES), F32)] * (2 * bunch), False)
        for i in range(bunch):
            q = first + i
            fin = row(FIN, q)
            h_r, h_i = ends[2 * i] * fin, ends[2 * i + 1] * fin
            for d, kind in enumerate((ONE, TWO, FOUR)):
                hop = 1 << d
                weight = jnp.where(sub >= hop, row(kind, q), 0.0)
                a_r, a_i = cmul(
                    pltpu.roll(h_r, hop, 0), pltpu.roll(h_i, hop, 0),
                    wide(base, 2 + 2 * d, q), wide(base, 3 + 2 * d, q),
                )
                h_r, h_i = h_r + weight * a_r, h_i + weight * a_i
            near_me[q : q + 1, :] = h_r[SEGS - 1 :]
            near_me[pairs + q : pairs + q + 1, :] = h_i[SEGS - 1 :]
            ref = row(REF, q)
            entry[0, q] = jnp.where(sub >= 1, pltpu.roll(h_r, 1, 0), 0.0) * ref
            entry[1, q] = jnp.where(sub >= 1, pltpu.roll(h_i, 1, 0), 0.0) * ref

    own_rows = pl.ds(WINDOW, rows)
    keys[own_rows, :] = project(KEY)

    def to_near(target):
        return pltpu.make_async_remote_copy(
            src_ref=near_me, dst_ref=near_me, send_sem=near_send.at[target], recv_sem=near_recv.at[mine],
            device_id={"sp": plane * inner + target}, device_id_type=MESH,
        )

    def from_near(source):
        return pltpu.make_async_remote_copy(
            src_ref=near_me, dst_ref=near.at[source], send_sem=near_send.at[source], recv_sem=near_recv.at[source],
            device_id={"sp": plane * inner + source}, device_id_type=MESH,
        )

    for hop in range(1, inner):
        to_near(lax.rem(mine + hop, inner)).start()
    values[own_rows, :] = project(VALUE)

    def halos(target):
        return [
            pltpu.make_async_remote_copy(
                src_ref=band.at[pl.ds(rows, WINDOW)], dst_ref=band.at[pl.ds(0, WINDOW)],
                send_sem=halo_send.at[k], recv_sem=halo_recv.at[k],
                device_id={"sp": target}, device_id_type=MESH,
            )
            for k, band in enumerate((keys, values))
        ]

    proj[0] = project(QUERY)

    @pl.when(me < count - 1)
    def _():
        for copy in halos(me + 1):
            copy.start()

    @pl.when(me == 0)
    def _():
        keys[:WINDOW, :] = jnp.zeros((WINDOW, keys.shape[1]), BF16)
        values[:WINDOW, :] = jnp.zeros((WINDOW, values.shape[1]), BF16)

    proj[1] = project(QUERY + 1)
    proj[2] = project(GATE)
    proj[3] = project(GATE + 1)

    blocks = rows // WINDOW
    group_size = Q_HEADS // KV_HEADS
    tile_heads = TILE // HEAD_DIM
    q_index = lax.broadcasted_iota(jnp.int32, (WINDOW, 2 * WINDOW), 0)
    k_index = lax.broadcasted_iota(jnp.int32, (WINDOW, 2 * WINDOW), 1)
    distance = WINDOW + q_index - k_index
    in_window = (distance >= 0) & (distance < WINDOW)

    def attend(block):
        here = pl.ds(block * WINDOW, WINDOW)
        band = pl.ds(block * WINDOW, 2 * WINDOW)
        allowed = in_window
        if block == 0:
            allowed = allowed & (k_index >= jnp.where(me == 0, WINDOW, 0))
        key, value = keys[band, :], values[band, :]
        for tile in range(2):
            query = proj[tile, here, :] * jnp.asarray(HEAD_DIM ** -0.5, BF16)
            results = []
            for j in range(tile_heads):
                head_id = tile * tile_heads + j
                kv = head_id // group_size
                k = key[:, kv * HEAD_DIM : (kv + 1) * HEAD_DIM]
                v = value[:, kv * HEAD_DIM : (kv + 1) * HEAD_DIM]
                scores = ntdot(query[:, j * HEAD_DIM : (j + 1) * HEAD_DIM], k)
                scores = jnp.where(allowed, scores, NEG_FILL)
                sink = sink_ref[head_id]
                maxima = jnp.maximum(jnp.max(scores, axis=-1, keepdims=True), sink)
                exponent = jnp.exp(scores - maxima)
                total = jnp.sum(exponent, axis=-1, keepdims=True) + jnp.exp(sink - maxima)
                results.append(ndot(exponent.astype(BF16), v) * (1.0 / total))
            gate = jax.nn.sigmoid(proj[2 + tile, here, :].astype(F32))
            head[here, pl.ds(tile * TILE, TILE)] = (gate * jnp.concatenate(results, axis=1)).astype(BF16)

    for block in range(1, blocks):
        attend(block)

    bd = lambda k: (base[k], base[k + 1])
    for hop in range(1, inner):
        from_near(lax.rem(mine + hop, inner)).wait_recv()
    agg_r = agg_i = jnp.zeros((pairs, LANES), F32)
    agg_s = jnp.zeros((1, LANES), F32)
    pw_r, pw_i = jnp.ones((pairs, LANES), F32), jnp.zeros((pairs, LANES), F32)
    pre = [agg_r, agg_i, agg_s, pw_r, pw_i]
    for i in range(inner):
        now = [agg_r, agg_i, agg_s, pw_r, pw_i]
        if i > 0:
            pre = [jnp.where(mine == i, a, b) for a, b in zip(now, pre)]
        shift_i = near[i, 2 * pairs : 2 * pairs + 1, :]
        a_r, a_i = cmul(agg_r, agg_i, block_r, block_i)
        factor = jnp.exp(per_pair(shift_i, pairs))
        agg_r = factor * a_r + near[i, :pairs, :]
        agg_i = factor * a_i + near[i, pairs : 2 * pairs, :]
        agg_s = agg_s + shift_i
        pw_r, pw_i = cmul(pw_r, pw_i, block_r, block_i)
    plane_r, plane_i = pw_r, pw_i
    far_me = far.at[plane]
    far_me[:pairs, :] = agg_r
    far_me[pairs : 2 * pairs, :] = agg_i
    far_me[2 * pairs :, :] = jnp.broadcast_to(agg_s, (SEGS, LANES))

    def to_far(target):
        return pltpu.make_async_remote_copy(
            src_ref=far_me, dst_ref=far_me, send_sem=far_send.at[target], recv_sem=far_recv.at[plane],
            device_id={"sp": target * inner + mine}, device_id_type=MESH,
        )

    def from_far(source):
        return pltpu.make_async_remote_copy(
            src_ref=far_me, dst_ref=far.at[source], send_sem=far_send.at[source], recv_sem=far_recv.at[source],
            device_id={"sp": source * inner + mine}, device_id_type=MESH,
        )

    before = jnp.exp(per_pair(pre[2], pairs))
    before_r, before_i = before * pre[3], before * pre[4]
    for q in range(pairs):
        spot = pl.ds(q * SEGS, SEGS)
        scale = row(PRE, q) * row(REF, q)
        init[0, q] = power[0, spot, :] * scale
        init[1, q] = power[1, spot, :] * scale

    for target in range(1, outer):
        @pl.when(plane < target)
        def _():
            to_far(target).start()

    for c in range(2):
        gate = project(SGATE + c)
        gate_ref[:, c * TILE : (c + 1) * TILE] = ndot(permute[...], gate).astype(BF16)

    @pl.when(me > 0)
    def _():
        for copy in halos(me):
            copy.wait_recv()

    attend(0)
    small[15].wait()
    width = how.shape[1] // 2
    pieces = away.shape[0]
    step = width // pieces

    def part_of(owner, piece):
        return pl.ds(pl.multiple_of(owner * width + piece * step, LANES), step)

    for piece in range(pieces):
        acc_other[piece] = ndot(head[...], how[:, part_of(other, piece)])
        acc_me[piece] = ndot(head[...], how[:, part_of(tp, piece)])

    carry_r = carry_i = jnp.zeros((pairs, LANES), F32)
    for z in range(outer - 1):
        @pl.when(z < plane)
        def _():
            from_far(z).wait_recv()

    for z in range(outer - 1):
        factor = jnp.exp(per_pair(far[z, 2 * pairs : 2 * pairs + 1, :], pairs))
        a_r, a_i = cmul(carry_r, carry_i, plane_r, plane_i)
        carry_r = jnp.where(z < plane, factor * a_r + far[z, :pairs, :], carry_r)
        carry_i = jnp.where(z < plane, factor * a_i + far[z, pairs : 2 * pairs, :], carry_i)
    in_r, in_i = cmul(carry_r, carry_i, before_r, before_i)
    in_r, in_i = in_r + pre[0], in_i + pre[1]
    zoh[0], zoh[1] = in_r, in_i
    for first in range(0, pairs, bunch):
        start = []
        for i in range(bunch):
            q = first + i
            s_r, s_i = cmul(init[0, q], init[1, q], wide(zoh, 0, q), wide(zoh, 1, q))
            start += [entry[0, q] + s_r, entry[1, q] + s_i]
        scan(first, start, True)
    for tile in range(tiles):
        lanes = pl.ds(tile * LANES, LANES)
        seen = sum(
            ntdot(states_ref[q], readout[q]) for q in range(tile * pairs_tile, (tile + 1) * pairs_tile)
        )
        recurrent = wout[:, lanes] * seen + skip_row[:, tile * LANES : (tile + 1) * LANES] * u_ref[:, lanes].astype(F32)
        gate = jax.nn.sigmoid(gate_ref[:, lanes].astype(F32))
        mixed[:, lanes] = (gate * jax.nn.gelu(recurrent)).astype(BF16)
    state = ndot(back[...], mixed[...]).astype(BF16)
    small[16].wait()

    copies = [
        pltpu.make_async_remote_copy(
            src_ref=away.at[piece], dst_ref=landed.at[piece],
            send_sem=out_send.at[piece], recv_sem=out_recv.at[piece],
            device_id={"tp": other}, device_id_type=MESH,
        )
        for piece in range(pieces)
    ]
    for piece in range(pieces):
        away[piece] = (acc_other[piece] + ndot(state, sow[:, part_of(other, piece)])).astype(BF16)
        if piece > 0:
            copies[piece - 1].start()
    held = acc_me[0] + ndot(state, sow[:, part_of(tp, 0)])
    copies[pieces - 1].start()
    for piece in range(pieces):
        total = held if piece == 0 else acc_me[piece] + ndot(state, sow[:, part_of(tp, piece)])
        copies[piece].wait()
        out_ref[:, pl.ds(piece * step, step)] = (total + landed[piece].astype(F32)).astype(BF16)

    for hop in range(1, inner):
        to_near(lax.rem(mine + hop, inner)).wait_send()
    for target in range(1, outer):
        @pl.when(plane < target)
        def _():
            to_far(target).wait_send()

    @pl.when(me < count - 1)
    def _():
        for copy in halos(me + 1):
            copy.wait_send()


def on_device(
    hidden, query_weight, key_weight, value_weight, head_gate_weight, state_in_weight, state_gate_weight,
    sink_logit, decay_real, decay_frequency, log_step, input_real, input_imaginary, output_real,
    output_imaginary, skip_weight, decay_shift, head_out_weight, state_out_weight,
):
    rows, half = hidden.shape
    groups, states = decay_real.shape
    pairs = groups // 2
    channels = groups * GROUP_CH
    count = lax.axis_size("sp")
    inner = 1 << (count.bit_length() // 2)
    outer = count // inner
    fixed = constants(rows, groups, states)
    tiles = sum(
        v.shape[1] for v in (
            query_weight, key_weight, value_weight, head_gate_weight, state_in_weight, state_gate_weight,
        )
    ) // TILE
    width = head_out_weight.shape[1] // 2
    pieces = 4
    small = (
        decay_real, decay_frequency, log_step.reshape(1, groups), input_real.transpose(0, 2, 1),
        input_imaginary.transpose(0, 2, 1), output_real, output_imaginary, skip_weight.T, decay_shift,
    )
    like = lambda v: pltpu.VMEM(v.shape, v.dtype)
    dma = pltpu.SemaphoreType.DMA
    scratch = [
        pltpu.VMEM((2, rows, half), BF16),
        pltpu.VMEM((tiles, 2 * half, TILE), BF16),
        like(head_out_weight), like(state_out_weight),
        *[like(v) for v in small],
        *[like(v) for v in fixed],
        pltpu.VMEM((pairs, LANES, TILE), BF16),
        pltpu.VMEM((pairs, LANES, TILE), BF16),
        pltpu.VMEM((pairs, rows, TILE), F32),
        pltpu.VMEM((pairs, rows, TILE), BF16),
        pltpu.VMEM((rows, channels), BF16),
        pltpu.VMEM((rows, channels), BF16),
        pltpu.VMEM((rows, channels), F32),
        pltpu.VMEM((rows, channels), F32),
        pltpu.VMEM((8, pairs, LANES), F32),
        pltpu.VMEM((2, pairs * SEGS, LANES), F32),
        pltpu.VMEM((7 * SEGS, groups * states), F32),
        pltpu.VMEM((2, pairs, LANES), F32),
        pltpu.VMEM((2, pairs, SEGS, LANES), F32),
        pltpu.VMEM((2, pairs, SEGS, LANES), F32),
        pltpu.VMEM((4, rows, TILE), BF16),
        pltpu.VMEM((WINDOW + rows, TILE), BF16),
        pltpu.VMEM((WINDOW + rows, TILE), BF16),
        pltpu.VMEM((rows, channels), BF16),
        pltpu.VMEM((rows, channels), BF16),
        pltpu.VMEM((inner, 2 * pairs + SEGS, LANES), F32),
        pltpu.VMEM((outer, 2 * pairs + SEGS, LANES), F32),
        pltpu.VMEM((pieces, rows, width // pieces), F32),
        pltpu.VMEM((pieces, rows, width // pieces), F32),
        pltpu.VMEM((pieces, rows, width // pieces), BF16),
        pltpu.VMEM((pieces, rows, width // pieces), BF16),
        dma((18,)), dma((tiles,)), dma, dma, dma((inner,)), dma((inner,)), dma((outer,)), dma((outer,)),
        dma((2,)), dma((2,)), dma((pieces,)), dma((pieces,)),
    ]
    return pl.pallas_call(
        layer_kernel,
        out_shape=jax.ShapeDtypeStruct((rows, width), BF16),
        in_specs=[ANY] * 7 + [SMEM] + [ANY] * (len(small) + 2 + len(fixed)),
        out_specs=VMEM,
        scratch_shapes=scratch,
        compiler_params=pltpu.CompilerParams(
            vmem_limit_bytes=60 * 1024 * 1024, collective_id=0, has_side_effects=True
        ),
        name="layer",
    )(
        hidden, query_weight, key_weight, value_weight, head_gate_weight, state_in_weight, state_gate_weight,
        sink_logit, *small, head_out_weight, state_out_weight, *fixed,
    )


def solution(mesh):
    in_specs = (
        P("sp", "tp"),
        P(None, "tp"),
        P(None, "tp"),
        P(None, "tp"),
        P(None, "tp"),
        P(None, "tp"),
        P(None, "tp"),
        P("tp"),
        P("tp", None),
        P("tp", None),
        P("tp"),
        P("tp", None, None),
        P("tp", None, None),
        P("tp", None, None),
        P("tp", None, None),
        P("tp", None),
        P("tp", "sp"),
        P("tp", None),
        P("tp", None),
    )
    out_specs = P("sp", "tp")
    return jax.shard_map(
        on_device, mesh=mesh, in_specs=in_specs, out_specs=out_specs, check_vma=False
    )
```

time: 76.7 us -> 28.9 us (0.38)
  the two profiles are of different devices: /device:TPU:25 before, /device:TPU:5 now
where the time goes in v1:
time: 28.9 us; the launch traced here: 28.8 us
  Pallas kernels  26.9 us (93%)
  local copies, waits for them, and re-layouts  1.87 us (6%)
    pallas_call x1, Pallas kernels, on_device(): pl.pallas_call(layer_kernel, out_shape=jax.ShapeDtypeStruct((rows, width)...  26.9 us
    unnamed x1, local copies, waits for them, and re-layouts  1.87 us

profile of v1, /device:TPU:5, one launch (start us, length us, event | category | flops | bytes accessed | tf_op | source)
XLA Modules:
  0.0 28.8 jit_solution(9591030020651134080)
XLA Ops:
  0.0 26.9 %layer.1 = bf16[256,1024]{1,0:T(8,128)(2,1)} custom-call(bf16[256,1024]{1,0:T(8,128)(2,1)} %hidden_ref.1, bf16[2048,512]{1,0:T(8,128)(2,1)} %wq_ref.1, bf16[2048,256]{1,0:T(8,128)(2,1)} %wk_ref.1, bf16[2048,256]{1,0:T(8,128)(2,1)} %wv_ref.1, bf16[2048,512]{1,0:T(8,128)(2,1)} %wg_ref.1, bf16[2048,512]{1,0:T(8,128)(2,1)} %wsi_ref.1, ...), custom_call_target="tpu_custom_call" | custom-call | tf_op jit(solution)/shard_map/layer/pallas_call | solution.py:594
  26.9 1.9 %copy.27 = bf16[256,1024]{1,0:T(8,128)(2,1)} copy(bf16[256,1024]{1,0:T(8,128)(2,1)} %layer.1) | data formatting | bytes 1048576

commit v2 on v1

--- a/solution.py
+++ b/solution.py
@@ -14,6 +14,8 @@
 LANES = 128
 SEGS = 8
 TILE = 256
+
+PREP_MIB, LAYER_MIB, ADD_MIB = 12, 36, 4
 
 NEG_FILL = -1e30
 MESH = pl.DeviceIdType.MESH
@@ -95,69 +97,55 @@
     return jnp.where(low, even, odd)
 
 
-def layer_kernel(
-    hidden_ref, wq_ref, wk_ref, wv_ref, wg_ref, wsi_ref, wsg_ref, sink_ref, dr_in, df_in, ls_in, ir_in, ii_in,
-    or_in, oi_in, skip_in, shift_in, how_ref, sow_ref, permute_in, back_in, running_in, sums_in, spread_in, widen_in,
-    out_ref,
-    x, w, how, sow, dr, df, ls, ir, ii, orr, oi, skip, shift, permute, back, running, sums, spread, widen,
-    drive, readout, pushed, states_ref, u_ref, gate_ref, win, wout, base, power, table, zoh, entry, init,
-    proj, keys, values, mixed, head, near, far, acc_me, acc_other, away, landed,
-    in_sem, w_sem, x_send, x_recv, near_send, near_recv, far_send, far_recv, halo_send, halo_recv, out_send, out_recv,
+def fetch_all(pairs_of, sems, first=0):
+    return [pltpu.make_async_copy(src, dst, sems.at[first + i]) for i, (src, dst) in enumerate(pairs_of)]
+
+
+def prepare_kernel(
+    hidden_ref, wsi_ref, wk_ref, wv_ref, dr_in, df_in, ls_in, shift_in, running_in, sums_in, spread_in, widen_in,
+    ir_in, ii_in, or_in, oi_in, skip_in,
+    x, w, drive, readout, win, wout, base, power, table, shift_rows, skip_row,
+    dr, df, ls, shift, running, sums, spread, widen, ir, ii, orr, oi, skip, zoh,
+    in_sem, w_sem, x_send, x_recv,
 ):
     tp = lax.axis_index("tp")
     other = 1 - tp
-    me = lax.axis_index("sp")
-    count = lax.axis_size("sp")
-    inner, outer = near.shape[0], far.shape[0]
-    mine, plane = lax.rem(me, inner), lax.div(me, inner)
-    rows, half_width = hidden_ref.shape
     pairs = drive.shape[0]
     groups = 2 * pairs
+    rows = win.shape[0]
     length = rows // SEGS
-    per_tile = LANES // GROUP_CH
-    tiles = groups // per_tile
-    pairs_tile = per_tile // 2
-
-    local = pltpu.make_async_copy
-    own_x = local(hidden_ref, x.at[tp], in_sem.at[0])
-    small = [
-        local(src, dst, in_sem.at[1 + i])
-        for i, (src, dst) in enumerate((
-            (dr_in, dr), (df_in, df), (ls_in, ls), (shift_in, shift), (running_in, running), (sums_in, sums),
-            (spread_in, spread), (widen_in, widen), (ir_in, ir), (ii_in, ii), (or_in, orr), (oi_in, oi),
-            (skip_in, skip), (permute_in, permute), (back_in, back), (how_ref, how), (sow_ref, sow),
-        ))
+    pairs_tile = LANES // GROUP_CH // 2
+    barrier = pltpu.get_barrier_semaphore()
+    pl.semaphore_signal(barrier, inc=1, device_id={"tp": other}, device_id_type=MESH)
+    own_x = pltpu.make_async_copy(hidden_ref, x.at[tp], in_sem.at[0])
+    own_x.start()
+    small = fetch_all((
+        (dr_in, dr), (df_in, df), (ls_in, ls), (shift_in, shift), (running_in, running), (sums_in, sums),
+        (spread_in, spread), (widen_in, widen), (ir_in, ir), (ii_in, ii), (or_in, orr), (oi_in, oi), (skip_in, skip),
+    ), in_sem, 1)
+    for copy in small:
+        copy.start()
+    columns = [
+        (ref.at[:, pl.ds(c * TILE, TILE)], w.at[i + c])
+        for ref, i in ((wsi_ref, 0), (wk_ref, 2), (wv_ref, 3)) for c in range(ref.shape[1] // TILE)
     ]
-    columns = []
-    for ref in (wsi_ref, wk_ref, wv_ref, wq_ref, wg_ref, wsg_ref):
-        for c in range(ref.shape[1] // TILE):
-            columns.append(ref.at[:, pl.ds(c * TILE, TILE)])
-    weights = [local(src, w.at[i], w_sem.at[i]) for i, src in enumerate(columns)]
-    own_x.start()
-    for copy in small[:-2]:
-        copy.start()
+    weights = fetch_all(columns, w_sem)
     for copy in weights:
         copy.start()
-    for copy in small[-2:]:
-        copy.start()
-
-    barrier = pltpu.get_barrier_semaphore()
-    pl.semaphore_signal(barrier, inc=1, device_id={"tp": other}, device_id_type=MESH)
-    for hop in range(1, inner):
-        target = plane * inner + lax.rem(mine + hop, inner)
-        pl.semaphore_signal(barrier, inc=1, device_id={"sp": target}, device_id_type=MESH)
-    for hop in range(1, outer):
-        target = lax.rem(plane + hop, outer) * inner + mine
-        pl.semaphore_signal(barrier, inc=1, device_id={"sp": target}, device_id_type=MESH)
-    for step in (1, count - 1):
-        target = lax.rem(me + step, count)
-        pl.semaphore_signal(barrier, inc=1, device_id={"sp": target}, device_id_type=MESH)
-
     zero = jnp.zeros((LANES, TILE), BF16)
     for q in range(pairs):
         drive[q] = zero
         readout[q] = zero
-    for copy in small[:3]:
+
+    pl.semaphore_wait(barrier, 1)
+    own_x.wait()
+    swap = pltpu.make_async_remote_copy(
+        src_ref=x.at[tp], dst_ref=x.at[tp], send_sem=x_send, recv_sem=x_recv,
+        device_id={"tp": other}, device_id_type=MESH,
+    )
+    swap.start()
+
+    for copy in small:
         copy.wait()
     two = lambda ref: jnp.concatenate(
         [ref[pl.ds(0, pairs, stride=2), :], ref[pl.ds(1, pairs, stride=2), :]], axis=1
@@ -175,32 +163,37 @@
     power_r, power_i = base_r, base_i
     for _ in range(length.bit_length() - 1):
         power_r, power_i = cmul(power_r, power_i, power_r, power_i)
-    for d in range(3):
+    for d in range(4):
         base[2 + 2 * d], base[3 + 2 * d] = power_r, power_i
+        if d == 0:
+            step_r, step_i = power_r, power_i
         power_r, power_i = cmul(power_r, power_i, power_r, power_i)
-    block_r, block_i = power_r, power_i
     run_r, run_i = jnp.ones_like(base_r), jnp.zeros_like(base_r)
     for k in range(SEGS):
         spot = pl.ds(k, pairs, stride=SEGS)
         power[0, spot, :] = run_r
         power[1, spot, :] = run_i
-        run_r, run_i = cmul(run_r, run_i, base[2], base[3])
-
-    for copy in small[3:8]:
-        copy.wait()
+        run_r, run_i = cmul(run_r, run_i, step_r, step_i)
+
     shifts = split(shift[...], 3)
     relative = sum(ntdot(running[...], piece) for piece in shifts)
+    totals = sum(ntdot(sums[...], piece) for piece in shifts)
     grown = jnp.concatenate(split(jnp.exp(-relative), 2), axis=1)
+    shrunk = jnp.concatenate(split(jnp.exp(relative), 2), axis=1)
+    scales = jnp.concatenate(split(jnp.exp(totals), 3), axis=1)
     win[...] = ndot(grown, spread[...])
-    shrunk = jnp.concatenate(split(jnp.exp(relative), 2), axis=1)
     wout[...] = ndot(shrunk, spread[...])
-    totals = sum(ntdot(sums[...], piece) for piece in shifts)
-    message_shift = totals[ALL * SEGS : (ALL + 1) * SEGS]
-    scales = jnp.concatenate(split(jnp.exp(totals), 3), axis=1)
     table[...] = ndot(scales, widen[...])
-
-    for copy in small[8:12]:
-        copy.wait()
+    shift_rows[...] = jnp.concatenate(
+        [totals[ALL * SEGS : (ALL + 1) * SEGS], jnp.zeros((SEGS, LANES - groups), F32)], axis=1
+    )
+    lanes_of = lax.broadcasted_iota(jnp.int32, (GROUP_CH, groups * GROUP_CH), 1) % GROUP_CH
+    channel = lax.broadcasted_iota(jnp.int32, (GROUP_CH, groups * GROUP_CH), 0)
+    skips = sum(ndot(piece, spread[:groups, :]) for piece in split(skip[...], 3))
+    skip_row[...] = jnp.broadcast_to(
+        jnp.sum(jnp.where(lanes_of == channel, skips, 0.0), axis=0, keepdims=True), skip_row.shape
+    )
+
     row_low = lax.broadcasted_iota(jnp.int32, (2 * GROUP_CH, LANES), 0) < GROUP_CH
     lane_low = lax.broadcasted_iota(jnp.int32, (2 * GROUP_CH, LANES), 1) < LANES // 2
     own_lane = row_low == lane_low
@@ -219,33 +212,67 @@
         readout[q, spot, :] = jnp.concatenate(
             [jnp.where(own_lane, pick(orr), 0.0), jnp.where(own_lane, -pick(oi), 0.0)], axis=1
         ).astype(BF16)
-
-    own_x.wait()
-    pl.semaphore_wait(barrier, inner + outer + 1)
-    swap = pltpu.make_async_remote_copy(
-        src_ref=x.at[tp], dst_ref=x.at[tp], send_sem=x_send, recv_sem=x_recv,
-        device_id={"tp": other}, device_id_type=MESH,
-    )
-    swap.start()
-    small[12].wait()
-    lanes_of = lax.broadcasted_iota(jnp.int32, (GROUP_CH, groups * GROUP_CH), 1) % GROUP_CH
-    channel = lax.broadcasted_iota(jnp.int32, (GROUP_CH, groups * GROUP_CH), 0)
-    skips = sum(ndot(piece, spread[:groups, :]) for piece in split(skip[...], 3))
-    skip_row = jnp.sum(jnp.where(lanes_of == channel, skips, 0.0), axis=0, keepdims=True)
-    small[13].wait()
-    small[14].wait()
     swap.wait()
-
-    def project(n):
-        weights[n].wait()
-        return (ndot(x[0], w[n, :half_width, :]) + ndot(x[1], w[n, half_width:, :])).astype(BF16)
-
-    SI, KEY, VALUE = 0, 2, 3
-    QUERY, GATE, SGATE = 4, 6, 8
-
+    for copy in weights:
+        copy.wait()
+
+
+def layer_kernel(
+    x, w, drive, readout, win, wout, base, power, table, shift_rows, skip_row,
+    wq_ref, wg_ref, wsg_ref, sink_in, how_ref, sow_ref, permute_in, back_in,
+    total_ref, landed,
+    w2, how, sow, permute, back, sink_ref,
+    pushed, states_ref, u_ref, gate_ref, carried, entry, init,
+    proj, keys, values, mixed, head, near, far, acc_me, acc_other, away,
+    in_sem, w_sem, near_send, near_recv, far_send, far_recv, halo_send, halo_recv, out_send, out_recv,
+):
+    tp = lax.axis_index("tp")
+    other = 1 - tp
+    me = lax.axis_index("sp")
+    count = lax.axis_size("sp")
+    inner, outer = near.shape[0], far.shape[0]
+    mine, plane = lax.rem(me, inner), lax.div(me, inner)
+    rows, half_width = x.shape[1:]
+    pairs = drive.shape[0]
+    groups = 2 * pairs
+    length = rows // SEGS
+    per_tile = LANES // GROUP_CH
+    tiles = groups // per_tile
+    pairs_tile = per_tile // 2
+
+    barrier = pltpu.get_barrier_semaphore()
+    for hop in range(1, inner):
+        target = plane * inner + lax.rem(mine + hop, inner)
+        pl.semaphore_signal(barrier, inc=1, device_id={"sp": target}, device_id_type=MESH)
+    for hop in range(1, outer):
+        target = lax.rem(plane + hop, outer) * inner + mine
+        pl.semaphore_signal(barrier, inc=1, device_id={"sp": target}, device_id_type=MESH)
+    for step in (1, count - 1):
+        target = lax.rem(me + step, count)
+        pl.semaphore_signal(barrier, inc=1, device_id={"sp": target}, device_id_type=MESH)
+    pl.semaphore_signal(barrier, inc=1, device_id={"tp": other}, device_id_type=MESH)
+
+    small = fetch_all(((permute_in, permute), (back_in, back), (sink_in, sink_ref), (how_ref, how), (sow_ref, sow)), in_sem)
+    columns = [
+        (ref.at[:, pl.ds(c * TILE, TILE)], w2.at[2 * i + c])
+        for i, ref in enumerate((wq_ref, wg_ref, wsg_ref)) for c in range(2)
+    ]
+    weights = fetch_all(columns, w_sem)
+    for copy in small[:3] + weights + small[3:]:
+        copy.start()
+
+    def project(block):
+        return (ndot(x[0], block[:half_width, :]) + ndot(x[1], block[half_width:, :])).astype(BF16)
+
+    small[0].wait()
+    small[1].wait()
+    own_rows = pl.ds(WINDOW, rows)
+    fed = [project(w[c]) for c in range(2)]
+    keys[own_rows, :] = project(w[2])
+    values[own_rows, :] = project(w[3])
     for c in range(2):
         lanes = pl.ds(c * TILE, TILE)
-        u = ndot(permute[...], project(SI + c))
+        u = ndot(permute[...], fed[c])
         u_ref[:, lanes] = u.astype(BF16)
         weighted = (u * win[:, lanes]).astype(BF16)
         for t in range(TILE // LANES):
@@ -254,6 +281,28 @@
             for i in range(pairs_tile):
                 q = tile * pairs_tile + i
                 pushed[q] = ndot(part, drive[q])
+
+    pl.semaphore_wait(barrier, inner + outer + 1)
+
+    def halos(target):
+        return [
+            pltpu.make_async_remote_copy(
+                src_ref=band.at[pl.ds(rows, WINDOW)], dst_ref=band.at[pl.ds(0, WINDOW)],
+                send_sem=halo_send.at[k], recv_sem=halo_recv.at[k],
+                device_id={"sp": target}, device_id_type=MESH,
+            )
+            for k, band in enumerate((keys, values))
+        ]
+
+    @pl.when(me < count - 1)
+    def _():
+        for copy in halos(me + 1):
+            copy.start()
+
+    @pl.when(me == 0)
+    def _():
+        keys[:WINDOW, :] = jnp.zeros((WINDOW, keys.shape[1]), BF16)
+        values[:WINDOW, :] = jnp.zeros((WINDOW, values.shape[1]), BF16)
 
     bunch = 8
 
@@ -292,9 +341,7 @@
 
     sub = lax.broadcasted_iota(jnp.int32, (SEGS, LANES), 0)
     near_me = near.at[mine]
-    near_me[2 * pairs :, :] = jnp.concatenate(
-        [message_shift, jnp.zeros((SEGS, LANES - groups), F32)], axis=1
-    )
+    near_me[2 * pairs :, :] = shift_rows[...]
     for first in range(0, pairs, bunch):
         ends = scan(first, [jnp.zeros((SEGS, LANES), F32)] * (2 * bunch), False)
         for i in range(bunch):
@@ -315,9 +362,6 @@
             entry[0, q] = jnp.where(sub >= 1, pltpu.roll(h_r, 1, 0), 0.0) * ref
             entry[1, q] = jnp.where(sub >= 1, pltpu.roll(h_i, 1, 0), 0.0) * ref
 
-    own_rows = pl.ds(WINDOW, rows)
-    keys[own_rows, :] = project(KEY)
-
     def to_near(target):
         return pltpu.make_async_remote_copy(
             src_ref=near_me, dst_ref=near_me, send_sem=near_send.at[target], recv_sem=near_recv.at[mine],
@@ -330,36 +374,14 @@
             device_id={"sp": plane * inner + source}, device_id_type=MESH,
         )
 
+    for copy in weights[:4]:
+        copy.wait()
     for hop in range(1, inner):
         to_near(lax.rem(mine + hop, inner)).start()
-    values[own_rows, :] = project(VALUE)
-
-    def halos(target):
-        return [
-            pltpu.make_async_remote_copy(
-                src_ref=band.at[pl.ds(rows, WINDOW)], dst_ref=band.at[pl.ds(0, WINDOW)],
-                send_sem=halo_send.at[k], recv_sem=halo_recv.at[k],
-                device_id={"sp": target}, device_id_type=MESH,
-            )
-            for k, band in enumerate((keys, values))
-        ]
-
-    proj[0] = project(QUERY)
-
-    @pl.when(me < count - 1)
-    def _():
-        for copy in halos(me + 1):
-            copy.start()
-
-    @pl.when(me == 0)
-    def _():
-        keys[:WINDOW, :] = jnp.zeros((WINDOW, keys.shape[1]), BF16)
-        values[:WINDOW, :] = jnp.zeros((WINDOW, values.shape[1]), BF16)
-
-    proj[1] = project(QUERY + 1)
-    proj[2] = project(GATE)
-    proj[3] = project(GATE + 1)
-
+    for n in range(4):
+        proj[n] = project(w2[n])
+
+    small[2].wait()
     blocks = rows // WINDOW
     group_size = Q_HEADS // KV_HEADS
     tile_heads = TILE // HEAD_DIM
@@ -396,9 +418,9 @@
     for block in range(1, blocks):
         attend(block)
 
-    bd = lambda k: (base[k], base[k + 1])
     for hop in range(1, inner):
         from_near(lax.rem(mine + hop, inner)).wait_recv()
+    block_r, block_i = base[8], base[9]
     agg_r = agg_i = jnp.zeros((pairs, LANES), F32)
     agg_s = jnp.zeros((1, LANES), F32)
     pw_r, pw_i = jnp.ones((pairs, LANES), F32), jnp.zeros((pairs, LANES), F32)
@@ -440,14 +462,16 @@
         init[0, q] = power[0, spot, :] * scale
         init[1, q] = power[1, spot, :] * scale
 
+    for copy in weights[4:]:
+        copy.wait()
     for target in range(1, outer):
         @pl.when(plane < target)
         def _():
             to_far(target).start()
 
+    gates = [project(w2[4 + c]) for c in range(2)]
     for c in range(2):
-        gate = project(SGATE + c)
-        gate_ref[:, c * TILE : (c + 1) * TILE] = ndot(permute[...], gate).astype(BF16)
+        gate_ref[:, c * TILE : (c + 1) * TILE] = ndot(permute[...], gates[c]).astype(BF16)
 
     @pl.when(me > 0)
     def _():
@@ -455,7 +479,8 @@
             copy.wait_recv()
 
     attend(0)
-    small[15].wait()
+    small[3].wait()
+    small[4].wait()
     width = how.shape[1] // 2
     pieces = away.shape[0]
     step = width // pieces
@@ -479,13 +504,12 @@
         carry_r = jnp.where(z < plane, factor * a_r + far[z, :pairs, :], carry_r)
         carry_i = jnp.where(z < plane, factor * a_i + far[z, pairs : 2 * pairs, :], carry_i)
     in_r, in_i = cmul(carry_r, carry_i, before_r, before_i)
-    in_r, in_i = in_r + pre[0], in_i + pre[1]
-    zoh[0], zoh[1] = in_r, in_i
+    carried[0], carried[1] = in_r + pre[0], in_i + pre[1]
     for first in range(0, pairs, bunch):
         start = []
         for i in range(bunch):
             q = first + i
-            s_r, s_i = cmul(init[0, q], init[1, q], wide(zoh, 0, q), wide(zoh, 1, q))
+            s_r, s_i = cmul(init[0, q], init[1, q], wide(carried, 0, q), wide(carried, 1, q))
             start += [entry[0, q] + s_r, entry[1, q] + s_i]
         scan(first, start, True)
     for tile in range(tiles):
@@ -493,11 +517,10 @@
         seen = sum(
             ntdot(states_ref[q], readout[q]) for q in range(tile * pairs_tile, (tile + 1) * pairs_tile)
         )
-        recurrent = wout[:, lanes] * seen + skip_row[:, tile * LANES : (tile + 1) * LANES] * u_ref[:, lanes].astype(F32)
+        recurrent = wout[:, lanes] * seen + skip_row[:1, lanes] * u_ref[:, lanes].astype(F32)
         gate = jax.nn.sigmoid(gate_ref[:, lanes].astype(F32))
         mixed[:, lanes] = (gate * jax.nn.gelu(recurrent)).astype(BF16)
     state = ndot(back[...], mixed[...]).astype(BF16)
-    small[16].wait()
 
     copies = [
         pltpu.make_async_remote_copy(
@@ -511,12 +534,10 @@
         away[piece] = (acc_other[piece] + ndot(state, sow[:, part_of(other, piece)])).astype(BF16)
         if piece > 0:
             copies[piece - 1].start()
-    held = acc_me[0] + ndot(state, sow[:, part_of(tp, 0)])
+    total_ref[0] = acc_me[0] + ndot(state, sow[:, part_of(tp, 0)])
     copies[pieces - 1].start()
-    for piece in range(pieces):
-        total = held if piece == 0 else acc_me[piece] + ndot(state, sow[:, part_of(tp, piece)])
-        copies[piece].wait()
-        out_ref[:, pl.ds(piece * step, step)] = (total + landed[piece].astype(F32)).astype(BF16)
+    for piece in range(1, pieces):
+        total_ref[piece] = acc_me[piece] + ndot(state, sow[:, part_of(tp, piece)])
 
     for hop in range(1, inner):
         to_near(lax.rem(mine + hop, inner)).wait_send()
@@ -529,6 +550,21 @@
     def _():
         for copy in halos(me + 1):
             copy.wait_send()
+    for copy in copies:
+        copy.wait()
+
+
+def add_kernel(total_ref, landed_ref, out_ref, stage, sem):
+    pieces, _, step = landed_ref.shape
+    copies = [
+        pltpu.make_async_copy(stage.at[piece], out_ref.at[:, pl.ds(piece * step, step)], sem.at[piece])
+        for piece in range(pieces)
+    ]
+    for piece in range(pieces):
+        stage[piece] = (total_ref[piece] + landed_ref[piece].astype(F32)).astype(BF16)
+        copies[piece].start()
+    for copy in copies:
+        copy.wait()
 
 
 def on_device(
@@ -543,68 +579,100 @@
     count = lax.axis_size("sp")
     inner = 1 << (count.bit_length() // 2)
     outer = count // inner
-    fixed = constants(rows, groups, states)
-    tiles = sum(
-        v.shape[1] for v in (
-            query_weight, key_weight, value_weight, head_gate_weight, state_in_weight, state_gate_weight,
-        )
-    ) // TILE
+    permute, back, running, sums, spread, widen = constants(rows, groups, states)
     width = head_out_weight.shape[1] // 2
     pieces = 4
+    like = lambda v: pltpu.VMEM(v.shape, v.dtype)
+    pin = lambda v: pltpu.with_memory_space_constraint(v, pltpu.HBM)
+    shaped = jax.ShapeDtypeStruct
+    dma = pltpu.SemaphoreType.DMA
+    mib = 1024 * 1024
     small = (
-        decay_real, decay_frequency, log_step.reshape(1, groups), input_real.transpose(0, 2, 1),
-        input_imaginary.transpose(0, 2, 1), output_real, output_imaginary, skip_weight.T, decay_shift,
-    )
-    like = lambda v: pltpu.VMEM(v.shape, v.dtype)
-    dma = pltpu.SemaphoreType.DMA
-    scratch = [
-        pltpu.VMEM((2, rows, half), BF16),
-        pltpu.VMEM((tiles, 2 * half, TILE), BF16),
-        like(head_out_weight), like(state_out_weight),
-        *[like(v) for v in small],
-        *[like(v) for v in fixed],
-        pltpu.VMEM((pairs, LANES, TILE), BF16),
-        pltpu.VMEM((pairs, LANES, TILE), BF16),
-        pltpu.VMEM((pairs, rows, TILE), F32),
-        pltpu.VMEM((pairs, rows, TILE), BF16),
-        pltpu.VMEM((rows, channels), BF16),
-        pltpu.VMEM((rows, channels), BF16),
-        pltpu.VMEM((rows, channels), F32),
-        pltpu.VMEM((rows, channels), F32),
-        pltpu.VMEM((8, pairs, LANES), F32),
-        pltpu.VMEM((2, pairs * SEGS, LANES), F32),
-        pltpu.VMEM((7 * SEGS, groups * states), F32),
-        pltpu.VMEM((2, pairs, LANES), F32),
-        pltpu.VMEM((2, pairs, SEGS, LANES), F32),
-        pltpu.VMEM((2, pairs, SEGS, LANES), F32),
-        pltpu.VMEM((4, rows, TILE), BF16),
-        pltpu.VMEM((WINDOW + rows, TILE), BF16),
-        pltpu.VMEM((WINDOW + rows, TILE), BF16),
-        pltpu.VMEM((rows, channels), BF16),
-        pltpu.VMEM((rows, channels), BF16),
-        pltpu.VMEM((inner, 2 * pairs + SEGS, LANES), F32),
-        pltpu.VMEM((outer, 2 * pairs + SEGS, LANES), F32),
-        pltpu.VMEM((pieces, rows, width // pieces), F32),
-        pltpu.VMEM((pieces, rows, width // pieces), F32),
-        pltpu.VMEM((pieces, rows, width // pieces), BF16),
-        pltpu.VMEM((pieces, rows, width // pieces), BF16),
-        dma((18,)), dma((tiles,)), dma, dma, dma((inner,)), dma((inner,)), dma((outer,)), dma((outer,)),
-        dma((2,)), dma((2,)), dma((pieces,)), dma((pieces,)),
-    ]
-    return pl.pallas_call(
+        decay_real, decay_frequency, log_step.reshape(1, groups), decay_shift, running, sums, spread, widen,
+        input_real.transpose(0, 2, 1), input_imaginary.transpose(0, 2, 1), output_real, output_imaginary,
+        skip_weight.T,
+    )
+    first_tiles = (state_in_weight.shape[1] + key_weight.shape[1] + value_weight.shape[1]) // TILE
+    prepared = (
+        shaped((2, rows, half), BF16),
+        shaped((first_tiles, 2 * half, TILE), BF16),
+        shaped((pairs, LANES, TILE), BF16),
+        shaped((pairs, LANES, TILE), BF16),
+        shaped((rows, channels), F32),
+        shaped((rows, channels), F32),
+        shaped((10, pairs, LANES), F32),
+        shaped((2, pairs * SEGS, LANES), F32),
+        shaped((7 * SEGS, groups * states), F32),
+        shaped((SEGS, LANES), F32),
+        shaped((SEGS, channels), F32),
+    )
+    ready = pl.pallas_call(
+        prepare_kernel,
+        out_shape=prepared,
+        in_specs=[ANY] * (4 + len(small)),
+        out_specs=(VMEM,) * len(prepared),
+        scratch_shapes=[
+            *[like(v) for v in small],
+            pltpu.VMEM((2, pairs, LANES), F32),
+            dma((1 + len(small),)), dma((first_tiles,)), dma, dma,
+        ],
+        compiler_params=pltpu.CompilerParams(
+            vmem_limit_bytes=PREP_MIB * mib, collective_id=0, has_side_effects=True
+        ),
+        name="prepare",
+    )(*map(pin, (hidden, state_in_weight, key_weight, value_weight, *small)))
+    total, landed = pl.pallas_call(
         layer_kernel,
-        out_shape=jax.ShapeDtypeStruct((rows, width), BF16),
-        in_specs=[ANY] * 7 + [SMEM] + [ANY] * (len(small) + 2 + len(fixed)),
-        out_specs=VMEM,
-        scratch_shapes=scratch,
+        out_shape=(
+            shaped((pieces, rows, width // pieces), F32),
+            shaped((pieces, rows, width // pieces), BF16),
+        ),
+        in_specs=[VMEM] * len(prepared) + [ANY] * 8,
+        out_specs=(VMEM, VMEM),
+        scratch_shapes=[
+            pltpu.VMEM((6, 2 * half, TILE), BF16),
+            like(head_out_weight), like(state_out_weight), like(permute), like(back),
+            pltpu.SMEM(sink_logit.shape, F32),
+            pltpu.VMEM((pairs, rows, TILE), F32),
+            pltpu.VMEM((pairs, rows, TILE), BF16),
+            pltpu.VMEM((rows, channels), BF16),
+            pltpu.VMEM((rows, channels), BF16),
+            pltpu.VMEM((2, pairs, LANES), F32),
+            pltpu.VMEM((2, pairs, SEGS, LANES), F32),
+            pltpu.VMEM((2, pairs, SEGS, LANES), F32),
+            pltpu.VMEM((4, rows, TILE), BF16),
+            pltpu.VMEM((WINDOW + rows, TILE), BF16),
+            pltpu.VMEM((WINDOW + rows, TILE), BF16),
+            pltpu.VMEM((rows, channels), BF16),
+            pltpu.VMEM((rows, channels), BF16),
+            pltpu.VMEM((inner, 2 * pairs + SEGS, LANES), F32),
+            pltpu.VMEM((outer, 2 * pairs + SEGS, LANES), F32),
+            pltpu.VMEM((pieces, rows, width // pieces), F32),
+            pltpu.VMEM((pieces, rows, width // pieces), F32),
+            pltpu.VMEM((pieces, rows, width // pieces), BF16),
+            dma((5,)), dma((6,)), dma((inner,)), dma((inner,)), dma((outer,)), dma((outer,)),
+            dma((2,)), dma((2,)), dma((pieces,)), dma((pieces,)),
+        ],
         compiler_params=pltpu.CompilerParams(
-            vmem_limit_bytes=60 * 1024 * 1024, collective_id=0, has_side_effects=True
+            vmem_limit_bytes=LAYER_MIB * mib, collective_id=1, has_side_effects=True
         ),
         name="layer",
     )(
-        hidden, query_weight, key_weight, value_weight, head_gate_weight, state_in_weight, state_gate_weight,
-        sink_logit, *small, head_out_weight, state_out_weight, *fixed,
-    )
+        *ready,
+        *map(pin, (
+            query_weight, head_gate_weight, state_gate_weight, sink_logit, head_out_weight, state_out_weight,
+            permute, back,
+        )),
+    )
+    return pl.pallas_call(
+        add_kernel,
+        out_shape=shaped((rows, width), BF16),
+        in_specs=[VMEM, VMEM],
+        out_specs=ANY,
+        scratch_shapes=[pltpu.VMEM((pieces, rows, width // pieces), BF16), dma((pieces,))],
+        compiler_params=pltpu.CompilerParams(vmem_limit_bytes=ADD_MIB * mib),
+        name="add",
+    )(total, landed)
 
 
 def solution(mesh):

time: 28.9 us -> 22.6 us (0.78)
  the two profiles are of different devices: /device:TPU:5 before, /device:TPU:25 now
where the time goes in v2:
time: 22.6 us; the launch traced here: 22.3 us
  Pallas kernels  22.3 us (99%)
    pallas_call x1, Pallas kernels, on_device(): pl.pallas_call(layer_kernel, out_shape=(shaped((pieces, rows, width // pi...  18 us
    pallas_call x1, Pallas kernels, on_device(): pl.pallas_call(prepare_kernel, out_shape=prepared, in_specs=[ANY] * (4 +...  3.41 us
    pallas_call x1, Pallas kernels, on_device(): pl.pallas_call(add_kernel, out_shape=shaped((rows, width), BF16), in_spec...  0.84 us

profile of v2, /device:TPU:25, one launch (start us, length us, event | category | flops | bytes accessed | tf_op | source)
XLA Modules:
  0.0 22.3 jit_solution(18437631061958767778)
XLA Ops:
  0.0 3.4 %prepare.1 = (bf16[2,256,1024]{2,1,0:T(8,128)(2,1)S(1)}, bf16[4,2048,256]{2,1,0:T(8,128)(2,1)S(1)}, bf16[16,128,256]{2,1,0:T(8,128)(2,1)S(1)}, bf16[16,128,256]{...) custom-call(bf16[256,1024]{1,0:T(8,128)(2,1)} %hidden_ref.1, ...), custom_call_target="tpu_custom_call" | custom-call | tf_op jit(solution)/shard_map/prepare/pallas_call | solution.py:609
  3.4 18.0 %layer.1 = (f32[4,256,256]{2,1,0:T(8,128)S(1)}, bf16[4,256,256]{2,1,0:T(8,128)(2,1)S(1)}) custom-call(bf16[2,256,1024]{2,1,0:T(8,128)(2,1)S(1)} %get-tuple-element.18.x, bf16[4,2048,256]{2,1,0:T(8,128)(2,1)S(1)} %get-tuple-element.19.w, bf16[16,128,256]{2,1,0:T(8,128)(2,1)S(1)} %get-tuple-element.20.drive, ...), custom_call_target="tpu_custom_call" | custom-call | tf_op jit(solution)/shard_map/layer/pallas_call | solution.py:624
  21.4 0.8 %add.1 = bf16[256,1024]{1,0:T(8,128)(2,1)} custom-call(f32[4,256,256]{2,1,0:T(8,128)S(1)} %get-tuple-element.29.total_ref, bf16[4,256,256]{2,1,0:T(8,128)(2,1)S(1)} %get-tuple-element.30.landed_ref), custom_call_target="tpu_custom_call" | custom-call | tf_op jit(solution)/shard_map/add/pallas_call | solution.py:667

commit v3 on v2

--- a/solution.py
+++ b/solution.py
@@ -15,7 +15,7 @@
 SEGS = 8
 TILE = 256
 
-PREP_MIB, LAYER_MIB, ADD_MIB = 12, 36, 4
+PREP_MIB, LAYER_MIB, CLOSE_MIB = 12, 36, 6
 
 NEG_FILL = -1e30
 MESH = pl.DeviceIdType.MESH
@@ -103,9 +103,9 @@
 
 def prepare_kernel(
     hidden_ref, wsi_ref, wk_ref, wv_ref, dr_in, df_in, ls_in, shift_in, running_in, sums_in, spread_in, widen_in,
-    ir_in, ii_in, or_in, oi_in, skip_in,
-    x, w, drive, readout, win, wout, base, power, table, shift_rows, skip_row,
-    dr, df, ls, shift, running, sums, spread, widen, ir, ii, orr, oi, skip, zoh,
+    ir_in, ii_in, permute_in,
+    x, w, drive, win, shrunk, base, power, table, shift_rows, permute, spread,
+    dr, df, ls, shift, running, sums, widen, ir, ii, zoh,
     in_sem, w_sem, x_send, x_recv,
 ):
     tp = lax.axis_index("tp")
@@ -121,7 +121,7 @@
     own_x.start()
     small = fetch_all((
         (dr_in, dr), (df_in, df), (ls_in, ls), (shift_in, shift), (running_in, running), (sums_in, sums),
-        (spread_in, spread), (widen_in, widen), (ir_in, ir), (ii_in, ii), (or_in, orr), (oi_in, oi), (skip_in, skip),
+        (spread_in, spread), (widen_in, widen), (ir_in, ir), (ii_in, ii), (permute_in, permute),
     ), in_sem, 1)
     for copy in small:
         copy.start()
@@ -131,11 +131,10 @@
     ]
     weights = fetch_all(columns, w_sem)
     for copy in weights:
-        copy.start()
+        copy.start(priority=1)
     zero = jnp.zeros((LANES, TILE), BF16)
     for q in range(pairs):
         drive[q] = zero
-        readout[q] = zero
 
     pl.semaphore_wait(barrier, 1)
     own_x.wait()
@@ -145,7 +144,7 @@
     )
     swap.start()
 
-    for copy in small:
+    for copy in small[:7]:
         copy.wait()
     two = lambda ref: jnp.concatenate(
         [ref[pl.ds(0, pairs, stride=2), :], ref[pl.ds(1, pairs, stride=2), :]], axis=1
@@ -179,20 +178,15 @@
     relative = sum(ntdot(running[...], piece) for piece in shifts)
     totals = sum(ntdot(sums[...], piece) for piece in shifts)
     grown = jnp.concatenate(split(jnp.exp(-relative), 2), axis=1)
-    shrunk = jnp.concatenate(split(jnp.exp(relative), 2), axis=1)
-    scales = jnp.concatenate(split(jnp.exp(totals), 3), axis=1)
+    shrunk[...] = jnp.concatenate(split(jnp.exp(relative), 2), axis=1)
     win[...] = ndot(grown, spread[...])
-    wout[...] = ndot(shrunk, spread[...])
-    table[...] = ndot(scales, widen[...])
     shift_rows[...] = jnp.concatenate(
         [totals[ALL * SEGS : (ALL + 1) * SEGS], jnp.zeros((SEGS, LANES - groups), F32)], axis=1
     )
-    lanes_of = lax.broadcasted_iota(jnp.int32, (GROUP_CH, groups * GROUP_CH), 1) % GROUP_CH
-    channel = lax.broadcasted_iota(jnp.int32, (GROUP_CH, groups * GROUP_CH), 0)
-    skips = sum(ndot(piece, spread[:groups, :]) for piece in split(skip[...], 3))
-    skip_row[...] = jnp.broadcast_to(
-        jnp.sum(jnp.where(lanes_of == channel, skips, 0.0), axis=0, keepdims=True), skip_row.shape
-    )
+    scales = jnp.concatenate(split(jnp.exp(totals), 3), axis=1)
+    for copy in small[7:]:
+        copy.wait()
+    table[...] = ndot(scales, widen[...])
 
     row_low = lax.broadcasted_iota(jnp.int32, (2 * GROUP_CH, LANES), 0) < GROUP_CH
     lane_low = lax.broadcasted_iota(jnp.int32, (2 * GROUP_CH, LANES), 1) < LANES // 2
@@ -209,22 +203,19 @@
         drive[q, spot, :] = jnp.concatenate(
             [jnp.where(own_lane, d_r, 0.0), jnp.where(own_lane, d_i, 0.0)], axis=1
         ).astype(BF16)
-        readout[q, spot, :] = jnp.concatenate(
-            [jnp.where(own_lane, pick(orr), 0.0), jnp.where(own_lane, -pick(oi), 0.0)], axis=1
-        ).astype(BF16)
     swap.wait()
     for copy in weights:
         copy.wait()
 
 
 def layer_kernel(
-    x, w, drive, readout, win, wout, base, power, table, shift_rows, skip_row,
-    wq_ref, wg_ref, wsg_ref, sink_in, how_ref, sow_ref, permute_in, back_in,
-    total_ref, landed,
-    w2, how, sow, permute, back, sink_ref,
+    x, w, drive, win, shrunk, base, power, table, shift_rows, permute, spread,
+    wq_ref, wg_ref, wsg_ref, sink_in, how_ref, sow_ref, back_in, or_in, oi_in, skip_in,
+    acc, state_x, sow_x,
+    w2, how, how_x, sow, back, sink_ref, orr, oi, skip, readout, wout, skip_row,
     pushed, states_ref, u_ref, gate_ref, carried, entry, init,
-    proj, keys, values, mixed, head, near, far, acc_me, acc_other, away,
-    in_sem, w_sem, near_send, near_recv, far_send, far_recv, halo_send, halo_recv, out_send, out_recv,
+    proj, keys, values, mixed, head, head_x, state, near, far,
+    in_sem, w_sem, near_send, near_recv, far_send, far_recv, halo_send, halo_recv, x_send, x_recv,
 ):
     tp = lax.axis_index("tp")
     other = 1 - tp
@@ -252,57 +243,48 @@
         pl.semaphore_signal(barrier, inc=1, device_id={"sp": target}, device_id_type=MESH)
     pl.semaphore_signal(barrier, inc=1, device_id={"tp": other}, device_id_type=MESH)
 
-    small = fetch_all(((permute_in, permute), (back_in, back), (sink_in, sink_ref), (how_ref, how), (sow_ref, sow)), in_sem)
+    pieces, _, step = acc.shape
+    width = pieces * step
+    half_of = lambda ref, owner: ref.at[:, pl.ds(pl.multiple_of(owner * width, LANES), width)]
+    small = fetch_all((
+        (sink_in, sink_ref), (or_in, orr), (oi_in, oi), (skip_in, skip), (back_in, back),
+        (half_of(how_ref, tp), how), (half_of(sow_ref, tp), sow),
+    ), in_sem)
     columns = [
         (ref.at[:, pl.ds(c * TILE, TILE)], w2.at[2 * i + c])
         for i, ref in enumerate((wq_ref, wg_ref, wsg_ref)) for c in range(2)
     ]
     weights = fetch_all(columns, w_sem)
-    for copy in small[:3] + weights + small[3:]:
+    for copy in small[:5] + weights + small[5:]:
         copy.start()
+
+    def cross(k, src, dst):
+        return pltpu.make_async_remote_copy(
+            src_ref=src, dst_ref=dst, send_sem=x_send.at[k], recv_sem=x_recv.at[k],
+            device_id={"tp": other}, device_id_type=MESH,
+        )
+
+    crossing = [cross(0, half_of(how_ref, other), how_x), cross(1, half_of(sow_ref, other), sow_x)]
+    head_cross, state_cross = cross(2, head, head_x), cross(3, state, state_x)
 
     def project(block):
         return (ndot(x[0], block[:half_width, :]) + ndot(x[1], block[half_width:, :])).astype(BF16)
 
-    small[0].wait()
-    small[1].wait()
     own_rows = pl.ds(WINDOW, rows)
     fed = [project(w[c]) for c in range(2)]
+    us = [ndot(permute[...], part) for part in fed]
     keys[own_rows, :] = project(w[2])
-    values[own_rows, :] = project(w[3])
     for c in range(2):
         lanes = pl.ds(c * TILE, TILE)
-        u = ndot(permute[...], fed[c])
-        u_ref[:, lanes] = u.astype(BF16)
-        weighted = (u * win[:, lanes]).astype(BF16)
+        u_ref[:, lanes] = us[c].astype(BF16)
+        weighted = (us[c] * win[:, lanes]).astype(BF16)
         for t in range(TILE // LANES):
             tile = c * (TILE // LANES) + t
             part = weighted[:, t * LANES : (t + 1) * LANES]
             for i in range(pairs_tile):
                 q = tile * pairs_tile + i
                 pushed[q] = ndot(part, drive[q])
-
-    pl.semaphore_wait(barrier, inner + outer + 1)
-
-    def halos(target):
-        return [
-            pltpu.make_async_remote_copy(
-                src_ref=band.at[pl.ds(rows, WINDOW)], dst_ref=band.at[pl.ds(0, WINDOW)],
-                send_sem=halo_send.at[k], recv_sem=halo_recv.at[k],
-                device_id={"sp": target}, device_id_type=MESH,
-            )
-            for k, band in enumerate((keys, values))
-        ]
-
-    @pl.when(me < count - 1)
-    def _():
-        for copy in halos(me + 1):
-            copy.start()
-
-    @pl.when(me == 0)
-    def _():
-        keys[:WINDOW, :] = jnp.zeros((WINDOW, keys.shape[1]), BF16)
-        values[:WINDOW, :] = jnp.zeros((WINDOW, values.shape[1]), BF16)
+    values[own_rows, :] = project(w[3])
 
     bunch = 8
 
@@ -362,26 +344,6 @@
             entry[0, q] = jnp.where(sub >= 1, pltpu.roll(h_r, 1, 0), 0.0) * ref
             entry[1, q] = jnp.where(sub >= 1, pltpu.roll(h_i, 1, 0), 0.0) * ref
 
-    def to_near(target):
-        return pltpu.make_async_remote_copy(
-            src_ref=near_me, dst_ref=near_me, send_sem=near_send.at[target], recv_sem=near_recv.at[mine],
-            device_id={"sp": plane * inner + target}, device_id_type=MESH,
-        )
-
-    def from_near(source):
-        return pltpu.make_async_remote_copy(
-            src_ref=near_me, dst_ref=near.at[source], send_sem=near_send.at[source], recv_sem=near_recv.at[source],
-            device_id={"sp": plane * inner + source}, device_id_type=MESH,
-        )
-
-    for copy in weights[:4]:
-        copy.wait()
-    for hop in range(1, inner):
-        to_near(lax.rem(mine + hop, inner)).start()
-    for n in range(4):
-        proj[n] = project(w2[n])
-
-    small[2].wait()
     blocks = rows // WINDOW
     group_size = Q_HEADS // KV_HEADS
     tile_heads = TILE // HEAD_DIM
@@ -415,8 +377,79 @@
             gate = jax.nn.sigmoid(proj[2 + tile, here, :].astype(F32))
             head[here, pl.ds(tile * TILE, TILE)] = (gate * jnp.concatenate(results, axis=1)).astype(BF16)
 
-    for block in range(1, blocks):
-        attend(block)
+    def middle():
+        for copy in weights[:4] + small[:1]:
+            copy.wait()
+        for n in range(4):
+            proj[n] = project(w2[n])
+        for block in range(1, blocks):
+            attend(block)
+
+    pl.when(me == 0)(middle)
+
+    def to_near(target):
+        return pltpu.make_async_remote_copy(
+            src_ref=near_me, dst_ref=near_me, send_sem=near_send.at[target], recv_sem=near_recv.at[mine],
+            device_id={"sp": plane * inner + target}, device_id_type=MESH,
+        )
+
+    def from_near(source):
+        return pltpu.make_async_remote_copy(
+            src_ref=near_me, dst_ref=near.at[source], send_sem=near_send.at[source], recv_sem=near_recv.at[source],
+            device_id={"sp": plane * inner + source}, device_id_type=MESH,
+        )
+
+    pl.semaphore_wait(barrier, inner + outer + 1)
+    for hop in range(1, inner):
+        to_near(lax.rem(mine + hop, inner)).start()
+
+    def halos(target):
+        return [
+            pltpu.make_async_remote_copy(
+                src_ref=band.at[pl.ds(rows, WINDOW)], dst_ref=band.at[pl.ds(0, WINDOW)],
+                send_sem=halo_send.at[k], recv_sem=halo_recv.at[k],
+                device_id={"sp": target}, device_id_type=MESH,
+            )
+            for k, band in enumerate((keys, values))
+        ]
+
+    @pl.when(me < count - 1)
+    def _():
+        for copy in halos(me + 1):
+            copy.start()
+
+    @pl.when(me == 0)
+    def _():
+        keys[:WINDOW, :] = jnp.zeros((WINDOW, keys.shape[1]), BF16)
+        values[:WINDOW, :] = jnp.zeros((WINDOW, values.shape[1]), BF16)
+
+    for copy in crossing:
+        copy.start()
+
+    pl.when(me != 0)(middle)
+
+    for copy in small[1:4]:
+        copy.wait()
+    wout[...] = ndot(shrunk[...], spread[...])
+    lanes_of = lax.broadcasted_iota(jnp.int32, (GROUP_CH, groups * GROUP_CH), 1) % GROUP_CH
+    channel = lax.broadcasted_iota(jnp.int32, (GROUP_CH, groups * GROUP_CH), 0)
+    skips = sum(ndot(piece, spread[:groups, :]) for piece in split(skip[...], 3))
+    skip_row[...] = jnp.broadcast_to(
+        jnp.sum(jnp.where(lanes_of == channel, skips, 0.0), axis=0, keepdims=True), skip_row.shape
+    )
+    row_low = lax.broadcasted_iota(jnp.int32, (2 * GROUP_CH, LANES), 0) < GROUP_CH
+    lane_low = lax.broadcasted_iota(jnp.int32, (2 * GROUP_CH, LANES), 1) < LANES // 2
+    own_lane = row_low == lane_low
+    zero = jnp.zeros((LANES, TILE), BF16)
+    for q in range(pairs):
+        pick = lambda ref: jnp.concatenate([
+            jnp.concatenate([ref[2 * q], ref[2 * q]], axis=1),
+            jnp.concatenate([ref[2 * q + 1], ref[2 * q + 1]], axis=1),
+        ], axis=0)
+        readout[q] = zero
+        readout[q, pl.ds((q % pairs_tile) * 2 * GROUP_CH, 2 * GROUP_CH), :] = jnp.concatenate(
+            [jnp.where(own_lane, pick(orr), 0.0), jnp.where(own_lane, -pick(oi), 0.0)], axis=1
+        ).astype(BF16)
 
     for hop in range(1, inner):
         from_near(lax.rem(mine + hop, inner)).wait_recv()
@@ -479,18 +512,13 @@
             copy.wait_recv()
 
     attend(0)
-    small[3].wait()
+    head_cross.start()
     small[4].wait()
-    width = how.shape[1] // 2
-    pieces = away.shape[0]
-    step = width // pieces
-
-    def part_of(owner, piece):
-        return pl.ds(pl.multiple_of(owner * width + piece * step, LANES), step)
-
+    small[5].wait()
+    small[6].wait()
+    part_of = lambda piece: pl.ds(piece * step, step)
     for piece in range(pieces):
-        acc_other[piece] = ndot(head[...], how[:, part_of(other, piece)])
-        acc_me[piece] = ndot(head[...], how[:, part_of(tp, piece)])
+        acc[piece] = ndot(head[...], how[:, part_of(piece)])
 
     carry_r = carry_i = jnp.zeros((pairs, LANES), F32)
     for z in range(outer - 1):
@@ -520,24 +548,15 @@
         recurrent = wout[:, lanes] * seen + skip_row[:1, lanes] * u_ref[:, lanes].astype(F32)
         gate = jax.nn.sigmoid(gate_ref[:, lanes].astype(F32))
         mixed[:, lanes] = (gate * jax.nn.gelu(recurrent)).astype(BF16)
-    state = ndot(back[...], mixed[...]).astype(BF16)
-
-    copies = [
-        pltpu.make_async_remote_copy(
-            src_ref=away.at[piece], dst_ref=landed.at[piece],
-            send_sem=out_send.at[piece], recv_sem=out_recv.at[piece],
-            device_id={"tp": other}, device_id_type=MESH,
+    state[...] = ndot(back[...], mixed[...]).astype(BF16)
+    state_cross.start()
+    crossing[0].wait()
+    head_cross.wait()
+    for piece in range(pieces):
+        acc[piece] += (
+            ndot(state[...], sow[:, part_of(piece)]) + ndot(head_x[...], how_x[:, part_of(piece)])
         )
-        for piece in range(pieces)
-    ]
-    for piece in range(pieces):
-        away[piece] = (acc_other[piece] + ndot(state, sow[:, part_of(other, piece)])).astype(BF16)
-        if piece > 0:
-            copies[piece - 1].start()
-    total_ref[0] = acc_me[0] + ndot(state, sow[:, part_of(tp, 0)])
-    copies[pieces - 1].start()
-    for piece in range(1, pieces):
-        total_ref[piece] = acc_me[piece] + ndot(state, sow[:, part_of(tp, piece)])
+    crossing[1].wait()
 
     for hop in range(1, inner):
         to_near(lax.rem(mine + hop, inner)).wait_send()
@@ -550,18 +569,17 @@
     def _():
         for copy in halos(me + 1):
             copy.wait_send()
-    for copy in copies:
-        copy.wait()
-
-
-def add_kernel(total_ref, landed_ref, out_ref, stage, sem):
-    pieces, _, step = landed_ref.shape
+    state_cross.wait()
+
+
+def close_kernel(acc, state_x, sow_x, out_ref, stage, sem):
+    pieces, _, step = acc.shape
     copies = [
         pltpu.make_async_copy(stage.at[piece], out_ref.at[:, pl.ds(piece * step, step)], sem.at[piece])
         for piece in range(pieces)
     ]
     for piece in range(pieces):
-        stage[piece] = (total_ref[piece] + landed_ref[piece].astype(F32)).astype(BF16)
+        stage[piece] = (acc[piece] + ndot(state_x[...], sow_x[:, pl.ds(piece * step, step)])).astype(BF16)
         copies[piece].start()
     for copy in copies:
         copy.wait()
@@ -589,22 +607,22 @@
     mib = 1024 * 1024
     small = (
         decay_real, decay_frequency, log_step.reshape(1, groups), decay_shift, running, sums, spread, widen,
-        input_real.transpose(0, 2, 1), input_imaginary.transpose(0, 2, 1), output_real, output_imaginary,
-        skip_weight.T,
-    )
+        input_real.transpose(0, 2, 1), input_imaginary.transpose(0, 2, 1), permute,
+    )
+    late = (output_real, output_imaginary, skip_weight.T)
     first_tiles = (state_in_weight.shape[1] + key_weight.shape[1] + value_weight.shape[1]) // TILE
     prepared = (
         shaped((2, rows, half), BF16),
         shaped((first_tiles, 2 * half, TILE), BF16),
         shaped((pairs, LANES, TILE), BF16),
-        shaped((pairs, LANES, TILE), BF16),
         shaped((rows, channels), F32),
-        shaped((rows, channels), F32),
+        shaped((rows, 2 * groups), BF16),
         shaped((10, pairs, LANES), F32),
         shaped((2, pairs * SEGS, LANES), F32),
         shaped((7 * SEGS, groups * states), F32),
         shaped((SEGS, LANES), F32),
-        shaped((SEGS, channels), F32),
+        shaped(permute.shape, BF16),
+        shaped(spread.shape, BF16),
     )
     ready = pl.pallas_call(
         prepare_kernel,
@@ -612,7 +630,7 @@
         in_specs=[ANY] * (4 + len(small)),
         out_specs=(VMEM,) * len(prepared),
         scratch_shapes=[
-            *[like(v) for v in small],
+            *[like(v) for v in small if v is not permute and v is not spread],
             pltpu.VMEM((2, pairs, LANES), F32),
             dma((1 + len(small),)), dma((first_tiles,)), dma, dma,
         ],
@@ -621,18 +639,24 @@
         ),
         name="prepare",
     )(*map(pin, (hidden, state_in_weight, key_weight, value_weight, *small)))
-    total, landed = pl.pallas_call(
+    closing = pl.pallas_call(
         layer_kernel,
         out_shape=(
             shaped((pieces, rows, width // pieces), F32),
-            shaped((pieces, rows, width // pieces), BF16),
+            shaped((rows, channels), BF16),
+            shaped((state_out_weight.shape[0], width), BF16),
         ),
-        in_specs=[VMEM] * len(prepared) + [ANY] * 8,
-        out_specs=(VMEM, VMEM),
+        in_specs=[VMEM] * len(prepared) + [ANY] * (7 + len(late)),
+        out_specs=(VMEM,) * 3,
         scratch_shapes=[
             pltpu.VMEM((6, 2 * half, TILE), BF16),
-            like(head_out_weight), like(state_out_weight), like(permute), like(back),
+            *[pltpu.VMEM((head_out_weight.shape[0], width), BF16)] * 3,
+            like(back),
             pltpu.SMEM(sink_logit.shape, F32),
+            *[like(v) for v in late],
+            pltpu.VMEM((pairs, LANES, TILE), BF16),
+            pltpu.VMEM((rows, channels), F32),
+            pltpu.VMEM((SEGS, channels), F32),
             pltpu.VMEM((pairs, rows, TILE), F32),
             pltpu.VMEM((pairs, rows, TILE), BF16),
             pltpu.VMEM((rows, channels), BF16),
@@ -643,15 +667,11 @@
             pltpu.VMEM((4, rows, TILE), BF16),
             pltpu.VMEM((WINDOW + rows, TILE), BF16),
             pltpu.VMEM((WINDOW + rows, TILE), BF16),
-            pltpu.VMEM((rows, channels), BF16),
-            pltpu.VMEM((rows, channels), BF16),
+            *[pltpu.VMEM((rows, channels), BF16)] * 4,
             pltpu.VMEM((inner, 2 * pairs + SEGS, LANES), F32),
             pltpu.VMEM((outer, 2 * pairs + SEGS, LANES), F32),
-            pltpu.VMEM((pieces, rows, width // pieces), F32),
-            pltpu.VMEM((pieces, rows, width // pieces), F32),
-            pltpu.VMEM((pieces, rows, width // pieces), BF16),
-            dma((5,)), dma((6,)), dma((inner,)), dma((inner,)), dma((outer,)), dma((outer,)),
-            dma((2,)), dma((2,)), dma((pieces,)), dma((pieces,)),
+            dma((7,)), dma((6,)), dma((inner,)), dma((inner,)), dma((outer,)), dma((outer,)),
+            dma((2,)), dma((2,)), dma((4,)), dma((4,)),
         ],
         compiler_params=pltpu.CompilerParams(
             vmem_limit_bytes=LAYER_MIB * mib, collective_id=1, has_side_effects=True
@@ -661,18 +681,18 @@
         *ready,
         *map(pin, (
             query_weight, head_gate_weight, state_gate_weight, sink_logit, head_out_weight, state_out_weight,
-            permute, back,
+            back, *late,
         )),
     )
     return pl.pallas_call(
-        add_kernel,
+        close_kernel,
         out_shape=shaped((rows, width), BF16),
-        in_specs=[VMEM, VMEM],
+        in_specs=[VMEM] * 3,
         out_specs=ANY,
         scratch_shapes=[pltpu.VMEM((pieces, rows, width // pieces), BF16), dma((pieces,))],
-        compiler_params=pltpu.CompilerParams(vmem_limit_bytes=ADD_MIB * mib),
-        name="add",
-    )(total, landed)
+        compiler_params=pltpu.CompilerParams(vmem_limit_bytes=CLOSE_MIB * mib),
+        name="close",
+    )(*closing)
 
 
 def solution(mesh):

time: 22.6 us -> 20.5 us (0.907)
  Pallas kernels: 22.3 us -> 20.3 us
    pallas_call x1, Pallas kernels: 18 us -> 15.8 us  [on_device(): pl.pallas_call(layer_kernel, out_shape=(shaped((pieces, rows, width // pi...]
    pallas_call x1, Pallas kernels: 0.84 us -> 1.19 us  [on_device(): pl.pallas_call(close_kernel, out_shape=shaped((rows, width), BF16), in_sp...]
where the time goes in v3:
time: 20.5 us; the launch traced here: 20.3 us
  Pallas kernels  20.3 us (99%)
    pallas_call x1, Pallas kernels, on_device(): pl.pallas_call(layer_kernel, out_shape=(shaped((pieces, rows, width // pi...  15.8 us
    pallas_call x1, Pallas kernels, on_device(): pl.pallas_call(prepare_kernel, out_shape=prepared, in_specs=[ANY] * (4 +...  3.29 us
    pallas_call x1, Pallas kernels, on_device(): pl.pallas_call(close_kernel, out_shape=shaped((rows, width), BF16), in_sp...  1.19 us

profile of v3, /device:TPU:25, one launch (start us, length us, event | category | flops | bytes accessed | tf_op | source)
XLA Modules:
  0.0 20.3 jit_solution(1387267487492311768)
XLA Ops:
  0.0 3.3 %prepare.1 = (bf16[2,256,1024]{2,1,0:T(8,128)(2,1)S(1)}, bf16[4,2048,256]{2,1,0:T(8,128)(2,1)S(1)}, bf16[16,128,256]{2,1,0:T(8,128)(2,1)S(1)}, f32[256,512]{1,0:...) custom-call(bf16[256,1024]{1,0:T(8,128)(2,1)} %hidden_ref.1, ...), custom_call_target="tpu_custom_call" | custom-call | tf_op jit(solution)/shard_map/prepare/pallas_call | solution.py:627
  3.3 15.8 %layer.1 = (f32[4,256,256]{2,1,0:T(8,128)S(1)}, bf16[256,512]{1,0:T(8,128)(2,1)S(1)}, bf16[512,1024]{1,0:T(8,128)(2,1)S(1)}) custom-call(bf16[2,256,1024]{2,1,0:T(8,128)(2,1)S(1)} %get-tuple-element.19.x, bf16[4,2048,256]{2,1,0:T(8,128)(2,1)S(1)} %get-tuple-element.20.w, bf16[16,128,256]{2,1,0:T(8,128)(2,1)S(1)} %get-tuple-element.21.drive, ...), custom_call_target="tpu_custom_call" | custom-call | tf_op jit(solution)/shard_map/layer/pallas_call | solution.py:642
  19.1 1.2 %close.1 = bf16[256,1024]{1,0:T(8,128)(2,1)} custom-call(f32[4,256,256]{2,1,0:T(8,128)S(1)} %get-tuple-element.30.acc, bf16[256,512]{1,0:T(8,128)(2,1)S(1)} %get-tuple-element.31.state_x, bf16[512,1024]{1,0:T(8,128)(2,1)S(1)} %get-tuple-element.32.sow_x), custom_call_target="tpu_custom_call" | custom-call | tf_op jit(solution)/shard_map/close/pallas_call | solution.py:687

commit v4 on v3

--- a/solution.py
+++ b/solution.py
@@ -99,6 +99,16 @@
 
 def fetch_all(pairs_of, sems, first=0):
     return [pltpu.make_async_copy(src, dst, sems.at[first + i]) for i, (src, dst) in enumerate(pairs_of)]
+
+
+def pack_shift(rows):
+    high, low = split(rows, 2)
+    return jnp.concatenate([high, low], axis=0)
+
+
+def unpack_shift(packed):
+    wide = packed.astype(F32)
+    return wide[:1] + wide[SEGS : SEGS + 1]
 
 
 def prepare_kernel(
@@ -211,11 +221,11 @@
 def layer_kernel(
     x, w, drive, win, shrunk, base, power, table, shift_rows, permute, spread,
     wq_ref, wg_ref, wsg_ref, sink_in, how_ref, sow_ref, back_in, or_in, oi_in, skip_in,
-    acc, state_x, sow_x,
-    w2, how, how_x, sow, back, sink_ref, orr, oi, skip, readout, wout, skip_row,
-    pushed, states_ref, u_ref, gate_ref, carried, entry, init,
-    proj, keys, values, mixed, head, head_x, state, near, far,
-    in_sem, w_sem, near_send, near_recv, far_send, far_recv, halo_send, halo_recv, x_send, x_recv,
+    acc, state_x, sow_x, head_x, how_x,
+    w2, how, sow, back, sink_ref, orr, oi, skip, readout, wout, skip_row,
+    pushed, states_ref, u_ref, gate_ref, carried, before, entry, init,
+    proj, keys, values, mixed, head, state, near, far,
+    in_sem, w_sem, near_send, near_recv, far_send, first_send, far_recv, halo_send, halo_recv, x_send, x_recv,
 ):
     tp = lax.axis_index("tp")
     other = 1 - tp
@@ -235,12 +245,15 @@
     for hop in range(1, inner):
         target = plane * inner + lax.rem(mine + hop, inner)
         pl.semaphore_signal(barrier, inc=1, device_id={"sp": target}, device_id_type=MESH)
-    for hop in range(1, outer):
-        target = lax.rem(plane + hop, outer) * inner + mine
-        pl.semaphore_signal(barrier, inc=1, device_id={"sp": target}, device_id_type=MESH)
-    for step in (1, count - 1):
-        target = lax.rem(me + step, count)
-        pl.semaphore_signal(barrier, inc=1, device_id={"sp": target}, device_id_type=MESH)
+
+    @pl.when(me > 0)
+    def _():
+        for hop in range(1, outer):
+            target = lax.rem(plane + hop, outer) * inner + mine
+            target = jnp.where(target == 0, 1, target)
+            pl.semaphore_signal(barrier, inc=1, device_id={"sp": target}, device_id_type=MESH)
+        pl.semaphore_signal(barrier, inc=1, device_id={"sp": me - 1}, device_id_type=MESH)
+
     pl.semaphore_signal(barrier, inc=1, device_id={"tp": other}, device_id_type=MESH)
 
     pieces, _, step = acc.shape
@@ -271,9 +284,30 @@
         return (ndot(x[0], block[:half_width, :]) + ndot(x[1], block[half_width:, :])).astype(BF16)
 
     own_rows = pl.ds(WINDOW, rows)
+    keys[own_rows, :] = project(w[2])
+    values[own_rows, :] = project(w[3])
     fed = [project(w[c]) for c in range(2)]
+
+    def halos(target):
+        return [
+            pltpu.make_async_remote_copy(
+                src_ref=band.at[pl.ds(rows, WINDOW)], dst_ref=band.at[pl.ds(0, WINDOW)],
+                send_sem=halo_send.at[k], recv_sem=halo_recv.at[k],
+                device_id={"sp": target}, device_id_type=MESH,
+            )
+            for k, band in enumerate((keys, values))
+        ]
+
+    signals = inner + jnp.where(me < count - 1, 1, 0) + jnp.where(me > 0, outer - 2, 0)
+    signals = signals + jnp.where(mine > 0, 1, 0) + jnp.where(me == 1, outer - 1, 0)
+
+    def send_halos():
+        @pl.when(me < count - 1)
+        def _():
+            for copy in halos(me + 1):
+                copy.start()
+
     us = [ndot(permute[...], part) for part in fed]
-    keys[own_rows, :] = project(w[2])
     for c in range(2):
         lanes = pl.ds(c * TILE, TILE)
         u_ref[:, lanes] = us[c].astype(BF16)
@@ -284,7 +318,6 @@
             for i in range(pairs_tile):
                 q = tile * pairs_tile + i
                 pushed[q] = ndot(part, drive[q])
-    values[own_rows, :] = project(w[3])
 
     bunch = 8
 
@@ -323,7 +356,7 @@
 
     sub = lax.broadcasted_iota(jnp.int32, (SEGS, LANES), 0)
     near_me = near.at[mine]
-    near_me[2 * pairs :, :] = shift_rows[...]
+    near_me[2 * pairs :, :] = pack_shift(shift_rows[...])
     for first in range(0, pairs, bunch):
         ends = scan(first, [jnp.zeros((SEGS, LANES), F32)] * (2 * bunch), False)
         for i in range(bunch):
@@ -338,8 +371,8 @@
                     wide(base, 2 + 2 * d, q), wide(base, 3 + 2 * d, q),
                 )
                 h_r, h_i = h_r + weight * a_r, h_i + weight * a_i
-            near_me[q : q + 1, :] = h_r[SEGS - 1 :]
-            near_me[pairs + q : pairs + q + 1, :] = h_i[SEGS - 1 :]
+            carried[0, q : q + 1, :] = h_r[SEGS - 1 :]
+            carried[1, q : q + 1, :] = h_i[SEGS - 1 :]
             ref = row(REF, q)
             entry[0, q] = jnp.where(sub >= 1, pltpu.roll(h_r, 1, 0), 0.0) * ref
             entry[1, q] = jnp.where(sub >= 1, pltpu.roll(h_i, 1, 0), 0.0) * ref
@@ -377,15 +410,20 @@
             gate = jax.nn.sigmoid(proj[2 + tile, here, :].astype(F32))
             head[here, pl.ds(tile * TILE, TILE)] = (gate * jnp.concatenate(results, axis=1)).astype(BF16)
 
-    def middle():
-        for copy in weights[:4] + small[:1]:
+    def last_part():
+        for copy in weights[4:]:
             copy.wait()
-        for n in range(4):
-            proj[n] = project(w2[n])
-        for block in range(1, blocks):
-            attend(block)
-
-    pl.when(me == 0)(middle)
+        gates = [project(w2[4 + c]) for c in range(2)]
+        for c in range(2):
+            gate_ref[:, c * TILE : (c + 1) * TILE] = ndot(permute[...], gates[c]).astype(BF16)
+
+    @pl.when(me == 0)
+    def _():
+        keys[:WINDOW, :] = jnp.zeros((WINDOW, keys.shape[1]), BF16)
+        values[:WINDOW, :] = jnp.zeros((WINDOW, values.shape[1]), BF16)
+
+    near_me[:pairs, :] = carried[0].astype(BF16)
+    near_me[pairs : 2 * pairs, :] = carried[1].astype(BF16)
 
     def to_near(target):
         return pltpu.make_async_remote_copy(
@@ -399,34 +437,19 @@
             device_id={"sp": plane * inner + source}, device_id_type=MESH,
         )
 
-    pl.semaphore_wait(barrier, inner + outer + 1)
+    pl.semaphore_wait(barrier, signals)
     for hop in range(1, inner):
         to_near(lax.rem(mine + hop, inner)).start()
 
-    def halos(target):
-        return [
-            pltpu.make_async_remote_copy(
-                src_ref=band.at[pl.ds(rows, WINDOW)], dst_ref=band.at[pl.ds(0, WINDOW)],
-                send_sem=halo_send.at[k], recv_sem=halo_recv.at[k],
-                device_id={"sp": target}, device_id_type=MESH,
-            )
-            for k, band in enumerate((keys, values))
-        ]
-
-    @pl.when(me < count - 1)
-    def _():
-        for copy in halos(me + 1):
-            copy.start()
-
-    @pl.when(me == 0)
-    def _():
-        keys[:WINDOW, :] = jnp.zeros((WINDOW, keys.shape[1]), BF16)
-        values[:WINDOW, :] = jnp.zeros((WINDOW, values.shape[1]), BF16)
-
-    for copy in crossing:
-        copy.start()
-
-    pl.when(me != 0)(middle)
+    crowded = mine == inner - 1
+    pl.when(jnp.logical_not(crowded))(send_halos)
+    for copy in weights[:4] + small[:1]:
+        copy.wait()
+    for n in range(4):
+        proj[n] = project(w2[n])
+    pl.when(crowded)(send_halos)
+    for block in range(1, blocks):
+        attend(block)
 
     for copy in small[1:4]:
         copy.wait()
@@ -451,35 +474,58 @@
             [jnp.where(own_lane, pick(orr), 0.0), jnp.where(own_lane, -pick(oi), 0.0)], axis=1
         ).astype(BF16)
 
-    for hop in range(1, inner):
-        from_near(lax.rem(mine + hop, inner)).wait_recv()
-    block_r, block_i = base[8], base[9]
-    agg_r = agg_i = jnp.zeros((pairs, LANES), F32)
-    agg_s = jnp.zeros((1, LANES), F32)
-    pw_r, pw_i = jnp.ones((pairs, LANES), F32), jnp.zeros((pairs, LANES), F32)
-    pre = [agg_r, agg_i, agg_s, pw_r, pw_i]
-    for i in range(inner):
-        now = [agg_r, agg_i, agg_s, pw_r, pw_i]
-        if i > 0:
-            pre = [jnp.where(mine == i, a, b) for a, b in zip(now, pre)]
-        shift_i = near[i, 2 * pairs : 2 * pairs + 1, :]
-        a_r, a_i = cmul(agg_r, agg_i, block_r, block_i)
-        factor = jnp.exp(per_pair(shift_i, pairs))
-        agg_r = factor * a_r + near[i, :pairs, :]
-        agg_i = factor * a_i + near[i, pairs : 2 * pairs, :]
-        agg_s = agg_s + shift_i
-        pw_r, pw_i = cmul(pw_r, pw_i, block_r, block_i)
-    plane_r, plane_i = pw_r, pw_i
+    def near_arrive():
+        for hop in range(1, inner):
+            from_near(lax.rem(mine + hop, inner)).wait_recv()
+
     far_me = far.at[plane]
-    far_me[:pairs, :] = agg_r
-    far_me[pairs : 2 * pairs, :] = agg_i
-    far_me[2 * pairs :, :] = jnp.broadcast_to(agg_s, (SEGS, LANES))
-
-    def to_far(target):
+
+    @pl.when(me == 0)
+    def _():
+        before[...] = jnp.zeros(before.shape, F32)
+
+    @pl.when(me > 0)
+    def _():
+        near_arrive()
+
+        block_r, block_i = base[8], base[9]
+        agg_r = agg_i = jnp.zeros((pairs, LANES), F32)
+        agg_s = jnp.zeros((1, LANES), F32)
+        pw_r, pw_i = jnp.ones((pairs, LANES), F32), jnp.zeros((pairs, LANES), F32)
+        pre = [agg_r, agg_i, agg_s, pw_r, pw_i]
+        for i in range(inner):
+            now = [agg_r, agg_i, agg_s, pw_r, pw_i]
+            if i > 0:
+                pre = [jnp.where(mine == i, a, b) for a, b in zip(now, pre)]
+            shift_i = unpack_shift(near[i, 2 * pairs :, :])
+            a_r, a_i = cmul(agg_r, agg_i, block_r, block_i)
+            factor = jnp.exp(per_pair(shift_i, pairs))
+            agg_r = factor * a_r + near[i, :pairs, :].astype(F32)
+            agg_i = factor * a_i + near[i, pairs : 2 * pairs, :].astype(F32)
+            agg_s = agg_s + shift_i
+            pw_r, pw_i = cmul(pw_r, pw_i, block_r, block_i)
+        far_me[:pairs, :] = agg_r.astype(BF16)
+        far_me[pairs : 2 * pairs, :] = agg_i.astype(BF16)
+        far_me[2 * pairs :, :] = pack_shift(jnp.broadcast_to(agg_s, (SEGS, LANES)))
+        scale = jnp.exp(per_pair(pre[2], pairs))
+        for k, value in enumerate((pre[0], pre[1], scale * pre[3], scale * pre[4], pw_r, pw_i)):
+            before[k] = value
+
+    def to_far(target, place, sem):
         return pltpu.make_async_remote_copy(
-            src_ref=far_me, dst_ref=far_me, send_sem=far_send.at[target], recv_sem=far_recv.at[plane],
-            device_id={"sp": target * inner + mine}, device_id_type=MESH,
+            src_ref=far_me, dst_ref=far_me, send_sem=sem.at[target], recv_sem=far_recv.at[plane],
+            device_id={"sp": target * inner + place}, device_id_type=MESH,
         )
+
+    def far_sends(act):
+        for target in range(1, outer):
+            @pl.when((plane < target) & (me > 0))
+            def _():
+                act(to_far(target, mine, far_send))
+
+            @pl.when(me == 1)
+            def _():
+                act(to_far(target, 0, first_send))
 
     def from_far(source):
         return pltpu.make_async_remote_copy(
@@ -487,38 +533,41 @@
             device_id={"sp": source * inner + mine}, device_id_type=MESH,
         )
 
-    before = jnp.exp(per_pair(pre[2], pairs))
-    before_r, before_i = before * pre[3], before * pre[4]
     for q in range(pairs):
         spot = pl.ds(q * SEGS, SEGS)
         scale = row(PRE, q) * row(REF, q)
         init[0, q] = power[0, spot, :] * scale
         init[1, q] = power[1, spot, :] * scale
 
-    for copy in weights[4:]:
+    far_sends(lambda copy: copy.start())
+    for copy in crossing:
+        copy.start()
+
+    last_part()
+
+    def first_block():
+        @pl.when(me > 0)
+        def _():
+            for copy in halos(me):
+                copy.wait_recv()
+
+        attend(0)
+
+    def head_out():
+        head_cross.start()
+        for piece in range(pieces):
+            acc[piece] = ndot(head[...], how[:, part_of(piece)])
+
+    for copy in small[4:]:
         copy.wait()
-    for target in range(1, outer):
-        @pl.when(plane < target)
-        def _():
-            to_far(target).start()
-
-    gates = [project(w2[4 + c]) for c in range(2)]
-    for c in range(2):
-        gate_ref[:, c * TILE : (c + 1) * TILE] = ndot(permute[...], gates[c]).astype(BF16)
-
-    @pl.when(me > 0)
+    part_of = lambda piece: pl.ds(piece * step, step)
+
+    soon = (lax.rem(me, 2) == 1) | (me == 0)
+
+    @pl.when(soon)
     def _():
-        for copy in halos(me):
-            copy.wait_recv()
-
-    attend(0)
-    head_cross.start()
-    small[4].wait()
-    small[5].wait()
-    small[6].wait()
-    part_of = lambda piece: pl.ds(piece * step, step)
-    for piece in range(pieces):
-        acc[piece] = ndot(head[...], how[:, part_of(piece)])
+        first_block()
+        head_out()
 
     carry_r = carry_i = jnp.zeros((pairs, LANES), F32)
     for z in range(outer - 1):
@@ -527,12 +576,12 @@
             from_far(z).wait_recv()
 
     for z in range(outer - 1):
-        factor = jnp.exp(per_pair(far[z, 2 * pairs : 2 * pairs + 1, :], pairs))
-        a_r, a_i = cmul(carry_r, carry_i, plane_r, plane_i)
-        carry_r = jnp.where(z < plane, factor * a_r + far[z, :pairs, :], carry_r)
-        carry_i = jnp.where(z < plane, factor * a_i + far[z, pairs : 2 * pairs, :], carry_i)
-    in_r, in_i = cmul(carry_r, carry_i, before_r, before_i)
-    carried[0], carried[1] = in_r + pre[0], in_i + pre[1]
+        factor = jnp.exp(per_pair(unpack_shift(far[z, 2 * pairs :, :]), pairs))
+        a_r, a_i = cmul(carry_r, carry_i, before[4], before[5])
+        carry_r = jnp.where(z < plane, factor * a_r + far[z, :pairs, :].astype(F32), carry_r)
+        carry_i = jnp.where(z < plane, factor * a_i + far[z, pairs : 2 * pairs, :].astype(F32), carry_i)
+    in_r, in_i = cmul(carry_r, carry_i, before[2], before[3])
+    carried[0], carried[1] = in_r + before[0], in_i + before[1]
     for first in range(0, pairs, bunch):
         start = []
         for i in range(bunch):
@@ -550,36 +599,40 @@
         mixed[:, lanes] = (gate * jax.nn.gelu(recurrent)).astype(BF16)
     state[...] = ndot(back[...], mixed[...]).astype(BF16)
     state_cross.start()
-    crossing[0].wait()
-    head_cross.wait()
+
+    @pl.when(jnp.logical_not(soon))
+    def _():
+        first_block()
+        head_out()
+
     for piece in range(pieces):
-        acc[piece] += (
-            ndot(state[...], sow[:, part_of(piece)]) + ndot(head_x[...], how_x[:, part_of(piece)])
-        )
-    crossing[1].wait()
-
+        acc[piece] += ndot(state[...], sow[:, part_of(piece)])
+    for copy in crossing:
+        copy.wait()
+    pl.when(me == 0)(near_arrive)
     for hop in range(1, inner):
         to_near(lax.rem(mine + hop, inner)).wait_send()
-    for target in range(1, outer):
-        @pl.when(plane < target)
-        def _():
-            to_far(target).wait_send()
+    far_sends(lambda copy: copy.wait_send())
 
     @pl.when(me < count - 1)
     def _():
         for copy in halos(me + 1):
             copy.wait_send()
+    head_cross.wait()
     state_cross.wait()
 
 
-def close_kernel(acc, state_x, sow_x, out_ref, stage, sem):
+def close_kernel(acc, state_x, sow_x, head_x, how_x, out_ref, stage, sem):
     pieces, _, step = acc.shape
     copies = [
         pltpu.make_async_copy(stage.at[piece], out_ref.at[:, pl.ds(piece * step, step)], sem.at[piece])
         for piece in range(pieces)
     ]
     for piece in range(pieces):
-        stage[piece] = (acc[piece] + ndot(state_x[...], sow_x[:, pl.ds(piece * step, step)])).astype(BF16)
+        lanes = pl.ds(piece * step, step)
+        stage[piece] = (
+            acc[piece] + ndot(head_x[...], how_x[:, lanes]) + ndot(state_x[...], sow_x[:, lanes])
+        ).astype(BF16)
         copies[piece].start()
     for copy in copies:
         copy.wait()
@@ -645,12 +698,14 @@
             shaped((pieces, rows, width // pieces), F32),
             shaped((rows, channels), BF16),
             shaped((state_out_weight.shape[0], width), BF16),
+            shaped((rows, head_out_weight.shape[0]), BF16),
+            shaped((head_out_weight.shape[0], width), BF16),
         ),
         in_specs=[VMEM] * len(prepared) + [ANY] * (7 + len(late)),
-        out_specs=(VMEM,) * 3,
+        out_specs=(VMEM,) * 5,
         scratch_shapes=[
             pltpu.VMEM((6, 2 * half, TILE), BF16),
-            *[pltpu.VMEM((head_out_weight.shape[0], width), BF16)] * 3,
+            *[pltpu.VMEM((head_out_weight.shape[0], width), BF16)] * 2,
             like(back),
             pltpu.SMEM(sink_logit.shape, F32),
             *[like(v) for v in late],
@@ -662,15 +717,16 @@
             pltpu.VMEM((rows, channels), BF16),
             pltpu.VMEM((rows, channels), BF16),
             pltpu.VMEM((2, pairs, LANES), F32),
+            pltpu.VMEM((6, pairs, LANES), F32),
             pltpu.VMEM((2, pairs, SEGS, LANES), F32),
             pltpu.VMEM((2, pairs, SEGS, LANES), F32),
             pltpu.VMEM((4, rows, TILE), BF16),
             pltpu.VMEM((WINDOW + rows, TILE), BF16),
             pltpu.VMEM((WINDOW + rows, TILE), BF16),
-            *[pltpu.VMEM((rows, channels), BF16)] * 4,
-            pltpu.VMEM((inner, 2 * pairs + SEGS, LANES), F32),
-            pltpu.VMEM((outer, 2 * pairs + SEGS, LANES), F32),
-            dma((7,)), dma((6,)), dma((inner,)), dma((inner,)), dma((outer,)), dma((outer,)),
+            *[pltpu.VMEM((rows, channels), BF16)] * 3,
+            pltpu.VMEM((inner, 2 * pairs + 2 * SEGS, LANES), BF16),
+            pltpu.VMEM((outer, 2 * pairs + 2 * SEGS, LANES), BF16),
+            dma((7,)), dma((6,)), dma((inner,)), dma((inner,)), *[dma((outer,))] * 3,
             dma((2,)), dma((2,)), dma((4,)), dma((4,)),
         ],
         compiler_params=pltpu.CompilerParams(
@@ -687,7 +743,7 @@
     return pl.pallas_call(
         close_kernel,
         out_shape=shaped((rows, width), BF16),
-        in_specs=[VMEM] * 3,
+        in_specs=[VMEM] * 5,
         out_specs=ANY,
         scratch_shapes=[pltpu.VMEM((pieces, rows, width // pieces), BF16), dma((pieces,))],
         compiler_params=pltpu.CompilerParams(vmem_limit_bytes=CLOSE_MIB * mib),

time: 20.5 us -> 20.4 us (level)
    pallas_call x1, Pallas kernels: 15.8 us -> 15.5 us  [on_device(): pl.pallas_call(layer_kernel, out_shape=(shaped((pieces, rows, width // pi...]
    pallas_call x1, Pallas kernels: 1.19 us -> 1.45 us  [on_device(): pl.pallas_call(close_kernel, out_shape=shaped((rows, width), BF16), in_sp...]
where the time goes in v4:
time: 20.4 us; the launch traced here: 20.3 us
  Pallas kernels  20.3 us (100%)
    pallas_call x1, Pallas kernels, on_device(): pl.pallas_call(layer_kernel, out_shape=(shaped((pieces, rows, width // pi...  15.5 us
    pallas_call x1, Pallas kernels, on_device(): pl.pallas_call(prepare_kernel, out_shape=prepared, in_specs=[ANY] * (4 +...  3.29 us
    pallas_call x1, Pallas kernels, on_device(): pl.pallas_call(close_kernel, out_shape=shaped((rows, width), BF16), in_sp...  1.45 us

profile of v4, /device:TPU:25, one launch (start us, length us, event | category | flops | bytes accessed | tf_op | source)
XLA Modules:
  0.0 20.3 jit_solution(11802191050141280910)
XLA Ops:
  0.0 3.3 %prepare.1 = (bf16[2,256,1024]{2,1,0:T(8,128)(2,1)S(1)}, bf16[4,2048,256]{2,1,0:T(8,128)(2,1)S(1)}, bf16[16,128,256]{2,1,0:T(8,128)(2,1)S(1)}, f32[256,512]{1,0:...) custom-call(bf16[256,1024]{1,0:T(8,128)(2,1)} %hidden_ref.1, ...), custom_call_target="tpu_custom_call" | custom-call | tf_op jit(solution)/shard_map/prepare/pallas_call | solution.py:680
  3.3 15.5 %layer.1 = (f32[4,256,256]{2,1,0:T(8,128)S(1)}, bf16[256,512]{1,0:T(8,128)(2,1)S(1)}, bf16[512,1024]{1,0:T(8,128)(2,1)S(1)}, bf16[256,512]{1,0:T(8,128)(2,1)S(1)}, bf16[512,1024]{1,0:T(8,128)(2,1)S(1)}) custom-call(bf16[2,256,1024]{2,1,0:T(8,128)(2,1)S(1)} %get-tuple-element.21.x, bf16[4,2048,256]{2,1,0:T(8,128)(2,1)S(1)} %get-tuple-element.22.w, ...), custom_call_target="tpu_custom_call" | custom-call | tf_op jit(solution)/shard_map/layer/pallas_call | solution.py:695
  18.8 1.4 %close.1 = bf16[256,1024]{1,0:T(8,128)(2,1)} custom-call(f32[4,256,256]{2,1,0:T(8,128)S(1)} %get-tuple-element.32.acc, bf16[256,512]{1,0:T(8,128)(2,1)S(1)} %get-tuple-element.33.state_x, bf16[512,1024]{1,0:T(8,128)(2,1)S(1)} %get-tuple-element.34.sow_x, bf16[256,512]{1,0:T(8,128)(2,1)S(1)} %get-tuple-element.35.head_x, ...), custom_call_target="tpu_custom_call" | custom-call | tf_op jit(solution)/shard_map/close/pallas_call | solution.py:743

commit v5 on v4

--- a/solution.py
+++ b/solution.py
@@ -250,7 +250,7 @@
     def _():
         for hop in range(1, outer):
             target = lax.rem(plane + hop, outer) * inner + mine
-            target = jnp.where(target == 0, 1, target)
+            target = jnp.where(target == 0, 2, target)
             pl.semaphore_signal(barrier, inc=1, device_id={"sp": target}, device_id_type=MESH)
         pl.semaphore_signal(barrier, inc=1, device_id={"sp": me - 1}, device_id_type=MESH)
 
@@ -299,7 +299,7 @@
         ]
 
     signals = inner + jnp.where(me < count - 1, 1, 0) + jnp.where(me > 0, outer - 2, 0)
-    signals = signals + jnp.where(mine > 0, 1, 0) + jnp.where(me == 1, outer - 1, 0)
+    signals = signals + jnp.where(mine > 0, 1, 0) + jnp.where(me == 2, outer - 1, 0)
 
     def send_halos():
         @pl.when(me < count - 1)
@@ -519,13 +519,13 @@
 
     def far_sends(act):
         for target in range(1, outer):
+            @pl.when(me == 2)
+            def _():
+                act(to_far(target, 0, first_send))
+
             @pl.when((plane < target) & (me > 0))
             def _():
                 act(to_far(target, mine, far_send))
-
-            @pl.when(me == 1)
-            def _():
-                act(to_far(target, 0, first_send))
 
     def from_far(source):
         return pltpu.make_async_remote_copy(
@@ -562,7 +562,7 @@
         copy.wait()
     part_of = lambda piece: pl.ds(piece * step, step)
 
-    soon = (lax.rem(me, 2) == 1) | (me == 0)
+    soon = halo_comes_soon(me)
 
     @pl.when(soon)
     def _():
@@ -609,6 +609,21 @@
         acc[piece] += ndot(state[...], sow[:, part_of(piece)])
     for copy in crossing:
         copy.wait()
+
+    @pl.when(soon)
+    def _():
+        head_cross.wait()
+        for piece in range(pieces):
+            acc[piece] += ndot(head_x[...], how_x[:, part_of(piece)])
+        state_cross.wait()
+
+    @pl.when(jnp.logical_not(soon))
+    def _():
+        state_cross.wait()
+        for piece in range(pieces):
+            acc[piece] += ndot(state_x[...], sow_x[:, part_of(piece)])
+        head_cross.wait()
+
     pl.when(me == 0)(near_arrive)
     for hop in range(1, inner):
         to_near(lax.rem(mine + hop, inner)).wait_send()
@@ -618,8 +633,10 @@
     def _():
         for copy in halos(me + 1):
             copy.wait_send()
-    head_cross.wait()
-    state_cross.wait()
+
+
+def halo_comes_soon(me):
+    return (lax.rem(me, 2) == 1) | (me == 0)
 
 
 def close_kernel(acc, state_x, sow_x, head_x, how_x, out_ref, stage, sem):
@@ -628,12 +645,15 @@
         pltpu.make_async_copy(stage.at[piece], out_ref.at[:, pl.ds(piece * step, step)], sem.at[piece])
         for piece in range(pieces)
     ]
-    for piece in range(pieces):
-        lanes = pl.ds(piece * step, step)
-        stage[piece] = (
-            acc[piece] + ndot(head_x[...], how_x[:, lanes]) + ndot(state_x[...], sow_x[:, lanes])
-        ).astype(BF16)
-        copies[piece].start()
+
+    def close(gated, weight):
+        for piece in range(pieces):
+            stage[piece] = (acc[piece] + ndot(gated[...], weight[:, pl.ds(piece * step, step)])).astype(BF16)
+            copies[piece].start()
+
+    soon = halo_comes_soon(lax.axis_index("sp"))
+    pl.when(soon)(lambda: close(state_x, sow_x))
+    pl.when(jnp.logical_not(soon))(lambda: close(head_x, how_x))
     for copy in copies:
         copy.wait()
 

time: 20.4 us -> 20.1 us (0.985)
  Pallas kernels: 20.3 us -> 20 us
    pallas_call x1, Pallas kernels: 1.45 us -> 1.2 us  [on_device(): pl.pallas_call(close_kernel, out_shape=shaped((rows, width), BF16), in_sp...]
where the time goes in v5:
time: 20.1 us; the launch traced here: 20 us
  Pallas kernels  20 us (100%)
    pallas_call x1, Pallas kernels, on_device(): pl.pallas_call(layer_kernel, out_shape=(shaped((pieces, rows, width // pi...  15.5 us
    pallas_call x1, Pallas kernels, on_device(): pl.pallas_call(prepare_kernel, out_shape=prepared, in_specs=[ANY] * (4 +...  3.29 us
    pallas_call x1, Pallas kernels, on_device(): pl.pallas_call(close_kernel, out_shape=shaped((rows, width), BF16), in_sp...  1.2 us

profile of v5, /device:TPU:25, one launch (start us, length us, event | category | flops | bytes accessed | tf_op | source)
XLA Modules:
  0.0 20.0 jit_solution(4575925664575982129)
XLA Ops:
  0.0 3.3 %prepare.1 = (bf16[2,256,1024]{2,1,0:T(8,128)(2,1)S(1)}, bf16[4,2048,256]{2,1,0:T(8,128)(2,1)S(1)}, bf16[16,128,256]{2,1,0:T(8,128)(2,1)S(1)}, f32[256,512]{1,0:...) custom-call(bf16[256,1024]{1,0:T(8,128)(2,1)} %hidden_ref.1, ...), custom_call_target="tpu_custom_call" | custom-call | tf_op jit(solution)/shard_map/prepare/pallas_call | solution.py:700
  3.3 15.5 %layer.1 = (f32[4,256,256]{2,1,0:T(8,128)S(1)}, bf16[256,512]{1,0:T(8,128)(2,1)S(1)}, bf16[512,1024]{1,0:T(8,128)(2,1)S(1)}, bf16[256,512]{1,0:T(8,128)(2,1)S(1)}, bf16[512,1024]{1,0:T(8,128)(2,1)S(1)}) custom-call(bf16[2,256,1024]{2,1,0:T(8,128)(2,1)S(1)} %get-tuple-element.21.x, bf16[4,2048,256]{2,1,0:T(8,128)(2,1)S(1)} %get-tuple-element.22.w, ...), custom_call_target="tpu_custom_call" | custom-call | tf_op jit(solution)/shard_map/layer/pallas_call | solution.py:715
  18.8 1.2 %close.1 = bf16[256,1024]{1,0:T(8,128)(2,1)} custom-call(f32[4,256,256]{2,1,0:T(8,128)S(1)} %get-tuple-element.32.acc, bf16[256,512]{1,0:T(8,128)(2,1)S(1)} %get-tuple-element.33.state_x, bf16[512,1024]{1,0:T(8,128)(2,1)S(1)} %get-tuple-element.34.sow_x, bf16[256,512]{1,0:T(8,128)(2,1)S(1)} %get-tuple-element.35.head_x, ...), custom_call_target="tpu_custom_call" | custom-call | tf_op jit(solution)/shard_map/close/pallas_call | solution.py:763

commit v6 on v5

--- a/solution.py
+++ b/solution.py
@@ -349,7 +349,7 @@
                         states_ref[first + i, spot, pl.ds(part * LANES, LANES)] = value
             return tuple(carry)
 
-        return lax.fori_loop(0, length // 2, steps, tuple(start), unroll=2)
+        return lax.fori_loop(0, length // 2, steps, tuple(start), unroll=2 if keep else 4)
 
     def row(kind, q):
         return table[kind * SEGS : (kind + 1) * SEGS, q * LANES : (q + 1) * LANES]

time: 20.1 us -> 20.1 us (level)
  no operation moved by 1% of the time
where the time goes in v6:
time: 20.1 us; the launch traced here: 20 us
  Pallas kernels  20 us (100%)
    pallas_call x1, Pallas kernels, on_device(): pl.pallas_call(layer_kernel, out_shape=(shaped((pieces, rows, width // pi...  15.5 us
    pallas_call x1, Pallas kernels, on_device(): pl.pallas_call(prepare_kernel, out_shape=prepared, in_specs=[ANY] * (4 +...  3.29 us
    pallas_call x1, Pallas kernels, on_device(): pl.pallas_call(close_kernel, out_shape=shaped((rows, width), BF16), in_sp...  1.2 us

profile of v6, /device:TPU:25, one launch (start us, length us, event | category | flops | bytes accessed | tf_op | source)
XLA Modules:
  0.0 20.0 jit_solution(10558530951118539305)
XLA Ops:
  0.0 3.3 %prepare.1 = (bf16[2,256,1024]{2,1,0:T(8,128)(2,1)S(1)}, bf16[4,2048,256]{2,1,0:T(8,128)(2,1)S(1)}, bf16[16,128,256]{2,1,0:T(8,128)(2,1)S(1)}, f32[256,512]{1,0:...) custom-call(bf16[256,1024]{1,0:T(8,128)(2,1)} %hidden_ref.1, ...), custom_call_target="tpu_custom_call" | custom-call | tf_op jit(solution)/shard_map/prepare/pallas_call | solution.py:700
  3.3 15.5 %layer.1 = (f32[4,256,256]{2,1,0:T(8,128)S(1)}, bf16[256,512]{1,0:T(8,128)(2,1)S(1)}, bf16[512,1024]{1,0:T(8,128)(2,1)S(1)}, bf16[256,512]{1,0:T(8,128)(2,1)S(1)}, bf16[512,1024]{1,0:T(8,128)(2,1)S(1)}) custom-call(bf16[2,256,1024]{2,1,0:T(8,128)(2,1)S(1)} %get-tuple-element.21.x, bf16[4,2048,256]{2,1,0:T(8,128)(2,1)S(1)} %get-tuple-element.22.w, ...), custom_call_target="tpu_custom_call" | custom-call | tf_op jit(solution)/shard_map/layer/pallas_call | solution.py:715
  18.8 1.2 %close.1 = bf16[256,1024]{1,0:T(8,128)(2,1)} custom-call(f32[4,256,256]{2,1,0:T(8,128)S(1)} %get-tuple-element.32.acc, bf16[256,512]{1,0:T(8,128)(2,1)S(1)} %get-tuple-element.33.state_x, bf16[512,1024]{1,0:T(8,128)(2,1)S(1)} %get-tuple-element.34.sow_x, bf16[256,512]{1,0:T(8,128)(2,1)S(1)} %get-tuple-element.35.head_x, ...), custom_call_target="tpu_custom_call" | custom-call | tf_op jit(solution)/shard_map/close/pallas_call | solution.py:763
